TPU v7x, 32 devices: a whole 2x2x4 slice. The times are simulated.
32 devices in a mesh: grp: 2 (over y), sp: 4 (over z), tp: 4 (over x, core).
Axes of the slice: x: 2, y: 2, z: 4, core: 2. Of those that a mesh axis runs over, the one named last changes fastest.
Arguments:
- tokens_in: bfloat16 [2048, 2048], P(('grp', 'sp')), parts along dimension 0, may hold values from -6 to 6
- input_gain: float32 [2048], replicated, may hold values from 0.1 to 1.9
- w_query: bfloat16 [2048, 1024], P('sp', 'tp'), may hold values from -0.125 to 0.125
- w_key: bfloat16 [2048, 1024], P('sp', 'tp'), may hold values from -1 to 1
- w_value: bfloat16 [2048, 1024], P('sp', 'tp'), may hold values from -0.125 to 0.125
- w_gates: bfloat16 [2048, 32], P('sp', 'tp'), may hold values from -3 to 3
- w_glu_value: bfloat16 [2048, 1024], P('sp', 'tp'), may hold values from -0.125 to 0.125
- sigmoid_opener_matrix: bfloat16 [2048, 1024], P('sp', 'tp'), may hold values from -0.125 to 0.125
- log_decay: float32 [2048, 16], P(('grp', 'sp'), 'tp'), parts along dimension 0, may hold values from -1 to 0
- head_gain: float32 [128], replicated, may hold values from 0.1 to 1.9
- conv_kernel: float32 [31, 1024], P(None, 'tp'), may hold values from -12 to 12
- norm_gain: float32 [1024], P('tp'), may hold values from 0.1 to 1.9
- norm_shift: float32 [1024], P('tp'), may hold values from -3 to 3
- out_delta: bfloat16 [2048, 1024], P(None, 'tp'), may hold values from -0.125 to 0.125
- out_conv: bfloat16 [2048, 1024], P(None, 'tp'), may hold values from -0.125 to 0.125
Outputs:
- mixed: bfloat16 [2048, 2048], P(('grp', 'sp'), 'tp'), parts along dimension 0
There are 2 independent parts, one for each index of `grp`. A program takes and returns all parts, laid end to end along the dimension named above; an argument that names none is the same for every part. Nothing has to cross between parts.
All inputs are finite; a program needn't handle non-finite values.
Results may differ from a plain program's by a relative error of at most 0.015.
Values may be sent and summed in bfloat16 or wider, within the bound.
No kernel may reach another device: no remote copies, remote signals or barrier semaphores. Data moves between devices by JAX's collectives and lax.ppermute only.
A program may use at most 64 MiB of HBM per device.

v0:
```python
import jax
import jax.numpy as jnp
from jax import lax
from jax.sharding import PartitionSpec as P

CONV_CH = 1024
BLOCK = 64


PRECISE = lax.Precision.HIGHEST
EPSILON = 1e-06
BETA_SHIFT = 6.0


def entering(value, axis, combine, identity, reverse):
    devices, place = (lax.axis_size(axis), lax.axis_index(axis))
    everything = jax.tree.map(
        lambda part, kind: lax.all_gather(part.astype(kind), axis),
        value,
        (jnp.bfloat16, jnp.bfloat16),
    )
    start = jax.tree.map(
        lambda part, zero: jnp.broadcast_to(jnp.asarray(zero, part.dtype), part.shape),
        value,
        identity,
    )

    def lap(k, before):
        at = devices - 1 - k if reverse else k
        reached = at > place if reverse else at < place
        new = combine(
            before, jax.tree.map(lambda part, own: part[at].astype(own.dtype), everything, value)
        )
        return jax.tree.map(lambda a, b: jnp.where(reached, a, b), new, before)

    return lax.fori_loop(0, devices, lap, start)


def with_halo(block, sides, width):
    for axis, dim in sides:
        count = lax.axis_size(axis)
        forward = [(i, i + 1) for i in range(count - 1)]
        backward = [(target, source) for source, target in forward]
        low = lax.ppermute(
            lax.slice_in_dim(block, block.shape[dim] - width, None, axis=dim), axis, forward
        )
        high = lax.ppermute(lax.slice_in_dim(block, 0, width, axis=dim), axis, backward)
        block = jnp.concatenate([low, block, high], axis=dim)
    return block


def high_dot(left, right):
    return jnp.matmul(left, right, precision=PRECISE)


def swap_last(tensor):
    return jnp.swapaxes(tensor, -1, -2)


def block_terms(query, key_rows, values, decay_log, beta_rate, block):
    head_count, length = (query.shape[0], query.shape[1])
    blocks = length // block

    def to_blocks(tensor):
        return tensor.reshape((head_count, blocks, block) + tensor.shape[2:])

    query, key_rows, values, decay_log, beta_rate = (
        to_blocks(tensor) for tensor in (query, key_rows, values, decay_log, beta_rate)
    )
    cumulative = jnp.cumsum(decay_log, axis=-1)
    positions = jnp.arange(block)
    on_or_below = positions[:, None] >= positions[None, :]
    strict = positions[:, None] > positions[None, :]
    log_gaps = cumulative[..., :, None] - cumulative[..., None, :]
    weighting = jnp.where(on_or_below, jnp.exp(jnp.where(on_or_below, log_gaps, 0.0)), 0.0)
    scaled_keys = key_rows * beta_rate[..., None]
    lower_part = jnp.where(strict, high_dot(scaled_keys, swap_last(key_rows)) * weighting, 0.0)
    identity = jnp.eye(block, dtype=jnp.float32)
    inverse = jax.scipy.linalg.solve_triangular(
        identity + lower_part,
        jnp.broadcast_to(identity, lower_part.shape),
        lower=True,
        unit_diagonal=True,
    )
    update = high_dot(inverse, values * beta_rate[..., None])
    mixed_keys = high_dot(inverse, scaled_keys * jnp.exp(cumulative)[..., None])
    in_block = jnp.where(on_or_below, high_dot(query, swap_last(key_rows)) * weighting, 0.0)
    q_decayed = query * jnp.exp(cumulative)[..., None]
    k_decayed = key_rows * jnp.exp(cumulative[..., -1:] - cumulative)[..., None]
    end_decay = jnp.exp(cumulative[..., -1])
    return tuple(
        (
            jnp.moveaxis(tensor, 1, 0)
            for tensor in (update, mixed_keys, in_block, q_decayed, k_decayed, end_decay)
        )
    )


def delta_local(query, key_rows, values, decay_log, beta_rate):
    stacked = block_terms(query, key_rows, values, decay_log, beta_rate, BLOCK)
    head_count, length, head_width = query.shape
    identity = jnp.broadcast_to(
        jnp.eye(head_width, dtype=jnp.float32), (head_count, head_width, head_width)
    )
    zero_state = jnp.zeros((head_count, head_width, values.shape[2]), jnp.float32)

    def advance(carry, pieces):
        state_now, carried = carry
        update, mixed_keys, in_block, q_decayed, k_decayed, end_decay = pieces
        new_values = update - high_dot(mixed_keys, state_now)
        output = high_dot(q_decayed, state_now) + high_dot(in_block, new_values)
        reading = high_dot(q_decayed - high_dot(in_block, mixed_keys), carried)
        passing = end_decay[:, None, None] * identity - high_dot(swap_last(k_decayed), mixed_keys)
        state_now = state_now * end_decay[:, None, None] + high_dot(
            swap_last(k_decayed), new_values
        )
        return ((state_now, high_dot(passing, carried)), (output, reading))

    (state_now, carried), (output, reading) = lax.scan(advance, (zero_state, identity), stacked)
    output = jnp.moveaxis(output, 0, 1).reshape(head_count, length, values.shape[2])
    reading = jnp.moveaxis(reading, 0, 1).reshape(head_count, length, head_width)
    return (output, reading, carried, state_now)


def chain(earlier, later):
    return (high_dot(later[0], earlier[0]), high_dot(later[0], earlier[1]) + later[1])


def reversed_rows(tensor):
    return jnp.flip(tensor, axis=1)


def delta_branch(query_proj, key_proj, value_proj, gate_proj, log_decay, head_gain):
    head_width = head_gain.shape[0]
    length = query_proj.shape[0]
    head_count = query_proj.shape[1] // head_width

    def by_head(tensor):
        return jnp.swapaxes(jax.nn.silu(tensor).reshape(length, head_count, head_width), 0, 1)

    def unit_rows(tensor):
        return tensor * lax.rsqrt(jnp.sum(tensor * tensor, axis=-1, keepdims=True) + EPSILON)

    query = unit_rows(by_head(query_proj)) * head_width ** (-0.5)
    key_rows = unit_rows(by_head(key_proj))
    values = by_head(value_proj)
    gate_parts = gate_proj.reshape(length, head_count, 4)
    rate_parts = log_decay.reshape(length, head_count, 2)
    decay_fore = jnp.swapaxes(
        rate_parts[:, :, 0] * (0.5 + jax.nn.sigmoid(gate_parts[:, :, 0])), 0, 1
    )
    beta_fore = jnp.swapaxes(jax.nn.sigmoid(gate_parts[:, :, 1] - BETA_SHIFT), 0, 1)
    decay_back = jnp.swapaxes(
        rate_parts[:, :, 1] * (0.5 + jax.nn.sigmoid(gate_parts[:, :, 2])), 0, 1
    )
    beta_back = jnp.swapaxes(jax.nn.sigmoid(gate_parts[:, :, 3] - BETA_SHIFT), 0, 1)
    identity = jnp.broadcast_to(
        jnp.eye(head_width, dtype=jnp.float32), (head_count, head_width, head_width)
    )
    zero_state = jnp.zeros((head_count, head_width, head_width), jnp.float32)
    forward_out, forward_read, forward_map, forward_end = delta_local(
        query, key_rows, values, decay_fore, beta_fore
    )
    forward_start = entering(
        (forward_map, forward_end), "sp", chain, (identity, zero_state), False
    )[1]
    back_out, back_read, back_map, back_end = delta_local(
        reversed_rows(query),
        reversed_rows(key_rows),
        reversed_rows(values),
        reversed_rows(decay_back),
        reversed_rows(beta_back),
    )
    back_start = entering((back_map, back_end), "sp", chain, (identity, zero_state), True)[1]
    joined = forward_out + high_dot(forward_read, forward_start)
    joined = joined + reversed_rows(back_out + high_dot(back_read, back_start))
    joined = (
        joined * lax.rsqrt(jnp.mean(joined * joined, axis=-1, keepdims=True) + EPSILON) * head_gain
    )
    return jnp.swapaxes(joined, 0, 1).reshape(length, head_count * head_width).astype(jnp.bfloat16)


def conv_branch(value_proj, gate_proj, conv_kernel, norm_gain, norm_shift):
    glu_rows = (value_proj * jax.nn.sigmoid(gate_proj)).astype(jnp.bfloat16)
    half_width = conv_kernel.shape[0] // 2
    length = glu_rows.shape[0]
    padded = with_halo(glu_rows, (("sp", 0),), half_width).astype(jnp.float32)
    conv_rows = padded[0:length] * conv_kernel[0]
    for offset in range(1, conv_kernel.shape[0]):
        conv_rows = conv_rows + padded[offset : offset + length] * conv_kernel[offset]
    row_sum, row_squares = lax.psum(
        (jnp.sum(conv_rows, axis=-1), jnp.sum(conv_rows * conv_rows, axis=-1)), "tp"
    )
    center = row_sum / CONV_CH
    spread = row_squares / CONV_CH - center * center
    normal_rows = (conv_rows - center[:, None]) * lax.rsqrt(spread + EPSILON)[:, None]
    return jax.nn.silu(normal_rows * norm_gain + norm_shift).astype(jnp.bfloat16)


def on_device(
    tokens_in,
    input_gain,
    w_query,
    w_key,
    w_value,
    w_gates,
    w_glu_value,
    sigmoid_opener_matrix,
    log_decay,
    head_gain,
    conv_kernel,
    norm_gain,
    norm_shift,
    out_delta,
    out_conv,
):
    rows = tokens_in.astype(jnp.float32)
    normed = (
        rows * lax.rsqrt(jnp.mean(rows * rows, axis=-1, keepdims=True) + EPSILON) * input_gain
    ).astype(jnp.bfloat16)
    weight_rows = (
        lax.all_gather(w_query, "sp", axis=0, tiled=True),
        lax.all_gather(w_key, "sp", axis=0, tiled=True),
        lax.all_gather(w_value, "sp", axis=0, tiled=True),
        lax.all_gather(w_gates, "sp", axis=0, tiled=True),
        lax.all_gather(w_glu_value, "sp", axis=0, tiled=True),
        lax.all_gather(sigmoid_opener_matrix, "sp", axis=0, tiled=True),
    )
    projected = tuple(
        (
            jnp.dot(normed, rows_here, preferred_element_type=jnp.float32)
            for rows_here in weight_rows
        )
    )
    delta_mix = delta_branch(
        projected[0], projected[1], projected[2], projected[3], log_decay, head_gain
    )
    filtered_blend = conv_branch(projected[4], projected[5], conv_kernel, norm_gain, norm_shift)
    contract = (((1,), (1,)), ((), ()))
    term = lax.dot_general(delta_mix, out_delta, contract, preferred_element_type=jnp.float32)
    term = term + lax.dot_general(
        filtered_blend, out_conv, contract, preferred_element_type=jnp.float32
    )
    return lax.psum_scatter(term.astype(jnp.bfloat16), "tp", scatter_dimension=1, tiled=True)


def solution(mesh):
    placed = (
        P(("grp", "sp"), None),
        P(),
        P("sp", "tp"),
        P("sp", "tp"),
        P("sp", "tp"),
        P("sp", "tp"),
        P("sp", "tp"),
        P("sp", "tp"),
        P(("grp", "sp"), "tp"),
        P(),
        P(None, "tp"),
        P("tp"),
        P("tp"),
        P(None, "tp"),
        P(None, "tp"),
    )
    return jax.shard_map(
        on_device, mesh=mesh, in_specs=placed, out_specs=P(("grp", "sp"), "tp"), check_vma=False
    )
```

profile of v0, /device:TPU:0, one launch (start us, length us, event | category | flops | bytes accessed | tf_op | source)
XLA Modules:
  0.0 307.7 jit_solution(15829972649994109252)
XLA Ops:
  6.6 0.7 all-gather.10.cloned.1.call-update
  7.3 0.7 all-gather.12.cloned.1.call-update
  8.1 0.7 all-gather.14.cloned.1.call-update
  10.4 14.9 %all_gather.42 = bf16[2048,8]{0,1:T(8,128)(2,1)S(1)} all-gather(bf16[512,8]{0,1:T(8,128)(2,1)S(1)} %copy-done.10), channel_id=1, replica_groups=mesh['grp'=2,'sp'=4,'tp'=4] {'sp'}, dimensions={0}, use_global_device_ids=true | all-gather | bytes 40960 | tf_op jit(solution)/shard_map/all_gather | solution.py:225
  27.7 0.7 fusion.211
  29.1 0.7 copy.84
  30.7 9.1 %all-gather.10.cloned.1.call-done = bf16[2048,256]{1,0:T(8,128)(2,1)} async-done(((bf16[512,256]{1,0:T(8,128)(2,1)}), bf16[2048,256]{1,0:T(8,128)(2,1)}) %all-gather.10.cloned.1.call-update) | async-done | bytes 1048592 | tf_op jit(solution)/shard_map/all_gather | solution.py:223
  39.8 1.9 divide_multiply_fusion.2
  43.0 39.3 %custom-call.8 = f32[2,4,1,64,64]{3,4,2,1,0:T(8,128)S(1)} custom-call(f32[2,4,1,64,64]{4,3,2,1,0:T(8,128)S(1)} %fusion.104), custom_call_target="InvertDiagBlocksLowerTriangular" | custom-call | tf_op jit(solution)/shard_map/jit(_solve_triangular)/vmap(vmap())/triangular_solve | solution.py:79
  82.9 2.2 divide_multiply_fusion.1
  85.9 1.1 convolution_bitcast_fusion.7
  87.2 10.9 %all-gather.14.cloned.1.call-done = bf16[2048,256]{1,0:T(8,128)(2,1)} async-done(((bf16[512,256]{1,0:T(8,128)(2,1)}), bf16[2048,256]{1,0:T(8,128)(2,1)}) %all-gather.14.cloned.1.call-update) | async-done | bytes 1048592 | tf_op jit(solution)/shard_map/all_gather | solution.py:222
  98.1 2.2 divide_multiply_fusion
  100.6 0.8 broadcast_multiply_fusion.1
  102.1 0.7 broadcast.121.clone2.2
  102.8 0.7 broadcast.121.clone2.3
  103.6 20.2 %while.64 = (s32[]{:T(128)}, f32[2,128,128]{2,1,0:T(8,128)S(1)}, f32[2,128,128]{2,1,0:T(8,128)S(1)}, f32[4,2,64,128]{3,2,0,1:T(8,128)}, f32[4,2,64,128]{3,2,0,1:...) while((s32[]{:T(128)}, f32[2,128,128]{2,1,0:T(8,128)S(1)}, ...), condition=%wide.region_5.7_spmd.clone, body=%wide.region_4.6_spmd.clone.sunk | while | flops 201605120 | bytes 2758829 | solution.py:119
  103.6 1.1 convolution_subtract_fusion.12
  104.9 0.8 fusion.320
  105.7 0.7 fusion.317
  107.1 0.9 fusion.321
  108.6 1.1 convolution_subtract_fusion.12
  110.0 0.8 fusion.320
  110.8 0.7 fusion.317
  112.1 0.9 fusion.321
  113.7 1.1 convolution_subtract_fusion.12
  115.0 0.8 fusion.320
  115.8 0.7 fusion.317
  117.1 0.9 fusion.321
  118.7 1.1 convolution_subtract_fusion.12
  120.0 0.8 fusion.320
  120.9 0.7 fusion.317
  122.2 0.9 fusion.321
  123.8 14.6 %all-gather = bf16[8,128,128]{2,1,0:T(8,128)(2,1)} all-gather(bf16[2,128,128]{2,1,0:T(8,128)(2,1)S(1)} %convert_element_type.96), channel_id=2, replica_groups=mesh['grp'=2,'sp'=4,'tp'=4] {'sp'}, dimensions={0}, use_global_device_ids=true | all-gather | bytes 327680 | tf_op jit(solution)/shard_map/all_gather | solution.py:18
  138.4 17.3 %all-gather.1 = bf16[8,128,128]{2,1,0:T(8,128)(2,1)} all-gather(bf16[2,128,128]{2,1,0:T(8,128)(2,1)S(1)} %convert_element_type.97), channel_id=3, replica_groups=mesh['grp'=2,'sp'=4,'tp'=4] {'sp'}, dimensions={0}, use_global_device_ids=true | all-gather | bytes 327680 | tf_op jit(solution)/shard_map/all_gather | solution.py:18
  155.7 1.8 copy.93
  158.1 39.3 %custom-call.9 = f32[2,4,1,64,64]{3,4,2,1,0:T(8,128)S(1)} custom-call(f32[2,4,1,64,64]{4,3,2,1,0:T(8,128)S(1)} %fusion.108), custom_call_target="InvertDiagBlocksLowerTriangular" | custom-call | tf_op jit(solution)/shard_map/jit(_solve_triangular)/vmap(vmap())/triangular_solve | solution.py:79
  200.3 0.7 broadcast.121.clone2
  201.0 14.3 %while.66 = (s32[]{:T(128)}, f32[2,128,128]{2,1,0:T(8,128)S(1)}, f32[2,128,128]{2,1,0:T(8,128)S(1)}, f32[4,2,64,128]{3,2,0,1:T(8,128)}, f32[4,2,64,128]{3,2,0,1:...) while((s32[]{:T(128)}, f32[2,128,128]{2,1,0:T(8,128)S(1)}, ...), condition=%wide.region_10.12_spmd.clone, body=%wide.region_9.11_spmd.clone.sunk | while | flops 201605120 | bytes 2758321 | solution.py:119
  201.5 0.8 fusion.344
  202.4 0.7 fusion.341
  205.1 0.8 fusion.344
  206.0 0.7 fusion.341
  208.7 0.8 fusion.344
  209.5 0.7 fusion.341
  212.3 0.8 fusion.344
  213.1 0.7 fusion.341
  215.4 14.0 %all-gather.2 = bf16[8,128,128]{2,1,0:T(8,128)(2,1)S(1)} all-gather(bf16[2,128,128]{2,1,0:T(8,128)(2,1)S(1)} %convert_element_type.98), channel_id=4, replica_groups=mesh['grp'=2,'sp'=4,'tp'=4] {'sp'}, dimensions={0}, use_global_device_ids=true | all-gather | bytes 327680 | tf_op jit(solution)/shard_map/all_gather | solution.py:18
  229.4 13.9 %all-gather.3 = bf16[8,128,128]{2,1,0:T(8,128)(2,1)S(1)} all-gather(bf16[2,128,128]{2,1,0:T(8,128)(2,1)S(1)} %convert_element_type.99), channel_id=5, replica_groups=mesh['grp'=2,'sp'=4,'tp'=4] {'sp'}, dimensions={0}, use_global_device_ids=true | all-gather | bytes 327680 | tf_op jit(solution)/shard_map/all_gather | solution.py:18
  243.3 1.1 while.67
  245.4 4.7 %while.65 = (s32[]{:T(128)}, f32[2,128,128]{2,1,0:T(8,128)S(1)}, s32[]{:T(128)}, bf16[4,2,128,128]{3,2,1,0:T(8,128)(2,1)}, bf16[4,2,128,128]{3,2,1,0:T(8,128)(2,1)}, /*index=5*/s32[]{:T(128)}, s32[]{:T(128)}) while((s32[]{:T(128)}, f32[2,128,128]{2,1,0:T(8,128)S(1)}, s32[]{:T(128)}, bf16[4,2,128,128]{3,2,1,0:T(8,128)(2,1)}, ...), condition=%wide.region_7.9_spmd.clone, body=%wide.region_6.8_spmd.clone.sunk | while | flops 50495492 | bytes 789087 | solution.py:36
  245.5 1.2 fusion.324
  246.7 1.1 fusion.324
  247.8 1.1 fusion.324
  249.0 1.1 fusion.324
  250.6 1.9 fusion.192
  252.6 1.9 fusion.113
  254.6 2.5 collective-permute-start
  257.1 1.3 collective-permute-start.1
  259.3 3.9 %collective-permute-done.1 = bf16[15,256]{0,1:T(8,128)(2,1)S(1)} collective-permute-done((bf16[15,256]{0,1:T(8,128)(2,1)S(1)}, bf16[15,256]{0,1:T(8,128)(2,1)S(1)}, u32[]{:S(2)}, u32[]{:S(2)}) %collective-permute-start.1) | collective-permute-done | bytes 7712 | tf_op jit(solution)/shard_map/ppermute | solution.py:47
  263.7 3.5 %fusion.208 = (f32[256]{0:T(256)S(1)}, f32[256]{0:T(256)S(1)}, f32[256,256]{0,1:T(8,128)S(1)}) fusion(f32[256]{0:T(256)S(1)} %bitcast.421, f32[286,256]{0,1:T(8,128)S(1)} %maximum_convert_fusion, f32[256]{0:T(256)S(1)} %bitcast.422, f32[256]{0:T(256)S(1)} %bitcast.393, f32[256]{0:T(256)S(1)} %bitcast.394, f32[256]{0:T(256)S(1)} %bitcast.395, ...), kind=kLoop, calls=%fused_computation.302 | loop fusion | flops 4193792 | bytes 8422400 | tf_op jit(solution)/shard_map/reduce_sum | solution.py:192
  267.2 5.7 %all-reduce = (f32[256]{0:T(256)S(1)}, f32[256]{0:T(256)S(1)}) all-reduce(f32[256]{0:T(256)S(1)} %get-tuple-element.565, f32[256]{0:T(256)S(1)} %get-tuple-element.564), channel_id=1, replica_groups=mesh['grp'=2,'sp'=4,'tp'=4] {'tp'}, use_global_device_ids=true, to_apply=%region_17.19 | all-reduce | flops 512 | bytes 4096 | tf_op jit(solution)/shard_map/psum | solution.py:191
  272.9 2.9 fusion.90
  275.8 25.1 %reduce-scatter.2.cloned.1.call-done = bf16[256,512]{1,0:T(8,128)(2,1)} async-done(((bf16[256,2048]{1,0:T(8,128)(2,1)}), bf16[256,512]{1,0:T(8,128)(2,1)}) %reduce-scatter.2.cloned.1.call-update) | async-done | bytes 262160 | tf_op jit(solution)/shard_map/reduce_scatter | solution.py:244
  (264 shorter events, 30.1 us)
Async XLA Ops:
  6.5 252.2 %copy-start = (bf16[2048,256]{1,0:T(8,128)(2,1)S(1)}, bf16[2048,256]{1,0:T(8,128)(2,1)}, u32[]{:S(2)}) copy-start(bf16[2048,256]{1,0:T(8,128)(2,1)} %param.38) | copy-start | bytes 3145732
  6.5 3.5 %copy-start.2 = (bf16[256,2048]{1,0:T(8,128)(2,1)S(1)}, bf16[256,2048]{1,0:T(8,128)(2,1)}, u32[]{:S(2)}) copy-start(bf16[256,2048]{1,0:T(8,128)(2,1)} %param.25) | copy-start | bytes 3145732
  6.5 3.8 %copy-start.10 = (bf16[512,8]{0,1:T(8,128)(2,1)S(1)}, bf16[512,8]{0,1:T(8,128)(2,1)}, u32[]{:S(2)}) copy-start(bf16[512,8]{0,1:T(8,128)(2,1)} %param.30) | copy-start | bytes 24580
  6.5 18.7 %copy-start.51 = (f32[2048]{0:T(1024)S(1)}, f32[2048]{0:T(1024)}, u32[]{:S(2)}) copy-start(f32[2048]{0:T(1024)} %param.26) | copy-start | bytes 24580
  6.5 33.3 %all-gather.10.cloned.1.call-start = ((), (), s32[]{:S(2)}) async-start(), calls=%async_computation.1 | async-start | bytes 1310720 | tf_op jit(solution)/shard_map/all_gather | solution.py:223
  7.3 18.4 %copy-start.44 = (f32[256,4]{0,1:T(4,128)S(1)}, f32[256,4]{0,1:T(4,128)}, u32[]{:S(2)}) copy-start(f32[256,4]{0,1:T(4,128)} %param.33) | copy-start | bytes 12292
  7.3 75.6 %all-gather.12.cloned.1.call-start = ((), (), s32[]{:S(2)}) async-start(), calls=%async_computation.2 | async-start | bytes 1310720 | tf_op jit(solution)/shard_map/all_gather | solution.py:224
  8.0 19.6 %copy-start.9 = (f32[31,256]{1,0:T(8,128)S(1)}, f32[31,256]{1,0:T(8,128)}, u32[]{:S(2)}) copy-start(f32[31,256]{1,0:T(8,128)} %param.35) | copy-start | bytes 95236
  8.0 90.0 %all-gather.14.cloned.1.call-start = ((), (), s32[]{:S(2)}) async-start(), calls=%async_computation.3 | async-start | bytes 1310720 | tf_op jit(solution)/shard_map/all_gather | solution.py:222
  8.8 241.8 %all-gather.16.cloned.1.call-start = ((), (), s32[]{:S(2)}) async-start(), calls=%async_computation.4 | async-start | bytes 1310720 | tf_op jit(solution)/shard_map/all_gather | solution.py:226
  9.4 243.2 %all-gather.18.cloned.1.call-start = ((), (), s32[]{:S(2)}) async-start(), calls=%async_computation.5 | async-start | bytes 1310720 | tf_op jit(solution)/shard_map/all_gather | solution.py:227
  9.9 290.9 %reduce-scatter.2.cloned.1.call-start = ((), (), s32[]{:S(2)}) async-start(), calls=%async_computation.6 | async-start | bytes 1310720 | tf_op jit(solution)/shard_map/reduce_scatter | solution.py:244
  10.0 32.3 %copy-start.7 = (f32[64,64]{1,0:T(8,128)}, f32[64,64]{1,0:T(8,128)S(1)}, u32[]{:S(2)}) copy-start(f32[64,64]{1,0:T(8,128)S(1)} %fusion.171) | copy-start | bytes 49156
  10.4 72.6 %copy-start.47 = (f32[256]{0:T(256)}, f32[256]{0:T(256)S(1)}, u32[]{:S(2)}) copy-start(f32[256]{0:T(256)S(1)} %add_rsqrt_fusion.4) | copy-start | bytes 3076
  29.1 13.2 %copy-start.11 = (pred[64,64]{1,0:T(8,128)(4,1)}, pred[64,64]{1,0:T(8,128)(4,1)S(1)}, u32[]{:S(2)}) copy-start(pred[64,64]{1,0:T(8,128)(4,1)S(1)} %get-tuple-element.690) | copy-start | bytes 12292
  85.2 12.9 %copy-start.48 = (f32[256]{0:T(256)S(1)}, f32[256]{0:T(256)}, u32[]{:S(2)}) copy-start(f32[256]{0:T(256)} %copy-done.47) | copy-start | bytes 3076
  85.2 12.9 %copy-start.52 = (f32[2048]{0:T(1024)S(1)}, f32[2048]{0:T(1024)}, u32[]{:S(2)}) copy-start(f32[2048]{0:T(1024)} %param.26) | copy-start | bytes 24580
  103.6 54.0 %copy-start.8 = (f32[64,64]{1,0:T(8,128)S(1)}, f32[64,64]{1,0:T(8,128)}, u32[]{:S(2)}) copy-start(f32[64,64]{1,0:T(8,128)} %copy-done.7) | copy-start | bytes 49156
  103.6 54.0 %copy-start.12 = (pred[64,64]{1,0:T(8,128)(4,1)S(1)}, pred[64,64]{1,0:T(8,128)(4,1)}, u32[]{:S(2)}) copy-start(pred[64,64]{1,0:T(8,128)(4,1)} %copy-done.11) | copy-start | bytes 12292
  157.5 41.9 %copy-start.1 = (f32[2,256,128]{2,1,0:T(8,128)S(1)}, f32[2,256,128]{2,1,0:T(8,128)}, u32[]{:S(2)}) copy-start(f32[2,256,128]{2,1,0:T(8,128)} %get-tuple-element.638) | copy-start | bytes 786436
  229.4 15.0 %copy-start.4 = (f32[4,2,64,128]{3,2,0,1:T(8,128)S(1)}, f32[4,2,64,128]{3,2,0,1:T(8,128)}, u32[]{:S(2)}) copy-start(f32[4,2,64,128]{3,2,0,1:T(8,128)} %get-tuple-element.367) | copy-start | bytes 786436
  245.0 5.1 %copy-start.5 = (f32[2,256,128]{1,2,0:T(8,128)S(1)}, f32[2,256,128]{1,2,0:T(8,128)}, u32[]{:S(2)}) copy-start(f32[2,256,128]{1,2,0:T(8,128)} %copy.93) | copy-start | bytes 786436
  245.0 5.1 %copy-start.6 = (f32[4,2,64,128]{3,2,0,1:T(8,128)S(1)}, f32[4,2,64,128]{3,2,0,1:T(8,128)}, u32[]{:S(2)}) copy-start(f32[4,2,64,128]{3,2,0,1:T(8,128)} %get-tuple-element.363) | copy-start | bytes 786436
  245.4 5.2 %copy-start.3 = (bf16[256,2048]{1,0:T(8,128)(2,1)S(1)}, bf16[256,2048]{1,0:T(8,128)(2,1)}, u32[]{:S(2)}) copy-start(bf16[256,2048]{1,0:T(8,128)(2,1)} %param.25) | copy-start | bytes 3145732
  245.4 5.2 %copy-start.49 = (f32[256]{0:T(256)S(1)}, f32[256]{0:T(256)}, u32[]{:S(2)}) copy-start(f32[256]{0:T(256)} %copy-done.47) | copy-start | bytes 3076
  245.4 5.2 %copy-start.53 = (f32[2048]{0:T(1024)S(1)}, f32[2048]{0:T(1024)}, u32[]{:S(2)}) copy-start(f32[2048]{0:T(1024)} %param.26) | copy-start | bytes 24580
  252.5 5.8 %copy-start.50 = (f32[128]{0:T(128)S(1)}, f32[128]{0:T(128)}, u32[]{:S(2)}) copy-start(f32[128]{0:T(128)} %param.34) | copy-start | bytes 1540
  254.6 4.7 %collective-permute-start = (bf16[15,256]{0,1:T(8,128)(2,1)S(1)}, bf16[15,256]{0,1:T(8,128)(2,1)S(1)}, u32[]{:S(2)}, u32[]{:S(2)}) collective-permute-start(bf16[15,256]{0,1:T(8,128)(2,1)S(1)} %get-tuple-element.639), channel_id=1, source_target_pairs={{0,4},{4,8},{8,12},{1,5},{5,9},{9,13},{2,6},{6,10},{10,14},{3,7},{... | collective-permute-start | bytes 23048 | tf_op jit(solution)/shard_map/ppermute | solution.py:44
  257.1 6.2 %collective-permute-start.1 = (bf16[15,256]{0,1:T(8,128)(2,1)S(1)}, bf16[15,256]{0,1:T(8,128)(2,1)S(1)}, u32[]{:S(2)}, u32[]{:S(2)}) collective-permute-start(bf16[15,256]{0,1:T(8,128)(2,1)S(1)} %get-tuple-element.640), channel_id=1, source_target_pairs={{4,0},{8,4},{12,8},{5,1},{9,5},{13,9},{6,2},{10,6},{14,10},{7,3},{... | collective-permute-start | bytes 23048 | tf_op jit(solution)/shard_map/ppermute | solution.py:47
  258.5 4.9 %copy-start.13 = (f32[1,256]{1,0:T(1,128)S(1)}, f32[1,256]{1,0:T(1,128)}, u32[]{:S(2)}) copy-start(f32[1,256]{1,0:T(1,128)} %get-tuple-element.641) | copy-start | bytes 3076
  258.5 4.9 %copy-start.14 = (f32[1,256]{1,0:T(1,128)S(1)}, f32[1,256]{1,0:T(1,128)}, u32[]{:S(2)}) copy-start(f32[1,256]{1,0:T(1,128)} %get-tuple-element.642) | copy-start | bytes 3076
  258.5 4.9 %copy-start.15 = (f32[1,256]{1,0:T(1,128)S(1)}, f32[1,256]{1,0:T(1,128)}, u32[]{:S(2)}) copy-start(f32[1,256]{1,0:T(1,128)} %get-tuple-element.643) | copy-start | bytes 3076
  258.5 4.9 %copy-start.16 = (f32[1,256]{1,0:T(1,128)S(1)}, f32[1,256]{1,0:T(1,128)}, u32[]{:S(2)}) copy-start(f32[1,256]{1,0:T(1,128)} %get-tuple-element.644) | copy-start | bytes 3076
  258.5 4.9 %copy-start.17 = (f32[1,256]{1,0:T(1,128)S(1)}, f32[1,256]{1,0:T(1,128)}, u32[]{:S(2)}) copy-start(f32[1,256]{1,0:T(1,128)} %get-tuple-element.645) | copy-start | bytes 3076
  258.5 4.9 %copy-start.18 = (f32[1,256]{1,0:T(1,128)S(1)}, f32[1,256]{1,0:T(1,128)}, u32[]{:S(2)}) copy-start(f32[1,256]{1,0:T(1,128)} %get-tuple-element.646) | copy-start | bytes 3076
  258.5 4.9 %copy-start.19 = (f32[1,256]{1,0:T(1,128)S(1)}, f32[1,256]{1,0:T(1,128)}, u32[]{:S(2)}) copy-start(f32[1,256]{1,0:T(1,128)} %get-tuple-element.647) | copy-start | bytes 3076
  258.5 4.9 %copy-start.20 = (f32[1,256]{1,0:T(1,128)S(1)}, f32[1,256]{1,0:T(1,128)}, u32[]{:S(2)}) copy-start(f32[1,256]{1,0:T(1,128)} %get-tuple-element.648) | copy-start | bytes 3076
  258.5 4.9 %copy-start.21 = (f32[1,256]{1,0:T(1,128)S(1)}, f32[1,256]{1,0:T(1,128)}, u32[]{:S(2)}) copy-start(f32[1,256]{1,0:T(1,128)} %get-tuple-element.649) | copy-start | bytes 3076
  258.6 4.9 %copy-start.22 = (f32[1,256]{1,0:T(1,128)S(1)}, f32[1,256]{1,0:T(1,128)}, u32[]{:S(2)}) copy-start(f32[1,256]{1,0:T(1,128)} %get-tuple-element.650) | copy-start | bytes 3076
  258.6 4.9 %copy-start.23 = (f32[1,256]{1,0:T(1,128)S(1)}, f32[1,256]{1,0:T(1,128)}, u32[]{:S(2)}) copy-start(f32[1,256]{1,0:T(1,128)} %get-tuple-element.651) | copy-start | bytes 3076
  258.6 4.9 %copy-start.24 = (f32[1,256]{1,0:T(1,128)S(1)}, f32[1,256]{1,0:T(1,128)}, u32[]{:S(2)}) copy-start(f32[1,256]{1,0:T(1,128)} %get-tuple-element.652) | copy-start | bytes 3076
  258.6 4.9 %copy-start.25 = (f32[1,256]{1,0:T(1,128)S(1)}, f32[1,256]{1,0:T(1,128)}, u32[]{:S(2)}) copy-start(f32[1,256]{1,0:T(1,128)} %get-tuple-element.653) | copy-start | bytes 3076
  258.6 4.9 %copy-start.26 = (f32[1,256]{1,0:T(1,128)S(1)}, f32[1,256]{1,0:T(1,128)}, u32[]{:S(2)}) copy-start(f32[1,256]{1,0:T(1,128)} %get-tuple-element.654) | copy-start | bytes 3076
  258.6 4.9 %copy-start.27 = (f32[1,256]{1,0:T(1,128)S(1)}, f32[1,256]{1,0:T(1,128)}, u32[]{:S(2)}) copy-start(f32[1,256]{1,0:T(1,128)} %get-tuple-element.655) | copy-start | bytes 3076
  258.6 4.9 %copy-start.28 = (f32[1,256]{1,0:T(1,128)S(1)}, f32[1,256]{1,0:T(1,128)}, u32[]{:S(2)}) copy-start(f32[1,256]{1,0:T(1,128)} %get-tuple-element.656) | copy-start | bytes 3076
  258.6 4.9 %copy-start.29 = (f32[1,256]{1,0:T(1,128)S(1)}, f32[1,256]{1,0:T(1,128)}, u32[]{:S(2)}) copy-start(f32[1,256]{1,0:T(1,128)} %get-tuple-element.657) | copy-start | bytes 3076
  258.6 4.9 %copy-start.30 = (f32[1,256]{1,0:T(1,128)S(1)}, f32[1,256]{1,0:T(1,128)}, u32[]{:S(2)}) copy-start(f32[1,256]{1,0:T(1,128)} %get-tuple-element.658) | copy-start | bytes 3076
  258.6 4.9 %copy-start.31 = (f32[1,256]{1,0:T(1,128)S(1)}, f32[1,256]{1,0:T(1,128)}, u32[]{:S(2)}) copy-start(f32[1,256]{1,0:T(1,128)} %get-tuple-element.659) | copy-start | bytes 3076
  258.7 4.9 %copy-start.32 = (f32[1,256]{1,0:T(1,128)S(1)}, f32[1,256]{1,0:T(1,128)}, u32[]{:S(2)}) copy-start(f32[1,256]{1,0:T(1,128)} %get-tuple-element.660) | copy-start | bytes 3076
  258.7 4.9 %copy-start.33 = (f32[1,256]{1,0:T(1,128)S(1)}, f32[1,256]{1,0:T(1,128)}, u32[]{:S(2)}) copy-start(f32[1,256]{1,0:T(1,128)} %get-tuple-element.661) | copy-start | bytes 3076
  258.7 4.9 %copy-start.34 = (f32[1,256]{1,0:T(1,128)S(1)}, f32[1,256]{1,0:T(1,128)}, u32[]{:S(2)}) copy-start(f32[1,256]{1,0:T(1,128)} %get-tuple-element.662) | copy-start | bytes 3076
  258.7 4.9 %copy-start.35 = (f32[1,256]{1,0:T(1,128)S(1)}, f32[1,256]{1,0:T(1,128)}, u32[]{:S(2)}) copy-start(f32[1,256]{1,0:T(1,128)} %get-tuple-element.663) | copy-start | bytes 3076
  258.7 4.9 %copy-start.36 = (f32[1,256]{1,0:T(1,128)S(1)}, f32[1,256]{1,0:T(1,128)}, u32[]{:S(2)}) copy-start(f32[1,256]{1,0:T(1,128)} %get-tuple-element.664) | copy-start | bytes 3076
  258.7 4.9 %copy-start.37 = (f32[1,256]{1,0:T(1,128)S(1)}, f32[1,256]{1,0:T(1,128)}, u32[]{:S(2)}) copy-start(f32[1,256]{1,0:T(1,128)} %get-tuple-element.665) | copy-start | bytes 3076
  258.7 4.9 %copy-start.38 = (f32[1,256]{1,0:T(1,128)S(1)}, f32[1,256]{1,0:T(1,128)}, u32[]{:S(2)}) copy-start(f32[1,256]{1,0:T(1,128)} %get-tuple-element.666) | copy-start | bytes 3076
  258.7 4.9 %copy-start.39 = (f32[1,256]{1,0:T(1,128)S(1)}, f32[1,256]{1,0:T(1,128)}, u32[]{:S(2)}) copy-start(f32[1,256]{1,0:T(1,128)} %get-tuple-element.667) | copy-start | bytes 3076
  258.7 4.9 %copy-start.40 = (f32[1,256]{1,0:T(1,128)S(1)}, f32[1,256]{1,0:T(1,128)}, u32[]{:S(2)}) copy-start(f32[1,256]{1,0:T(1,128)} %get-tuple-element.668) | copy-start | bytes 3076
  258.7 4.9 %copy-start.41 = (f32[1,256]{1,0:T(1,128)S(1)}, f32[1,256]{1,0:T(1,128)}, u32[]{:S(2)}) copy-start(f32[1,256]{1,0:T(1,128)} %get-tuple-element.669) | copy-start | bytes 3076
  258.8 4.9 %copy-start.42 = (f32[1,256]{1,0:T(1,128)S(1)}, f32[1,256]{1,0:T(1,128)}, u32[]{:S(2)}) copy-start(f32[1,256]{1,0:T(1,128)} %get-tuple-element.670) | copy-start | bytes 3076
  258.8 4.9 %copy-start.43 = (f32[1,256]{1,0:T(1,128)S(1)}, f32[1,256]{1,0:T(1,128)}, u32[]{:S(2)}) copy-start(f32[1,256]{1,0:T(1,128)} %get-tuple-element.671) | copy-start | bytes 3076
  263.7 9.3 %copy-start.45 = (f32[256]{0:T(256)S(1)}, f32[256]{0:T(256)}, u32[]{:S(2)}) copy-start(f32[256]{0:T(256)} %param.37) | copy-start | bytes 3076
  263.7 9.2 %copy-start.46 = (f32[256]{0:T(256)S(1)}, f32[256]{0:T(256)}, u32[]{:S(2)}) copy-start(f32[256]{0:T(256)} %param.36) | copy-start | bytes 3076
Sparse Core Ops, SparseCore 0:
  8.9 30.8 all-gather.9
  41.4 27.5 all-gather.11
  70.5 27.4 all-gather.13
  99.5 27.1 all-gather.15
  128.1 31.9 all-gather.17
  275.9 24.8 reduce-scatter.1
where the time goes:
time: 309 us; the launch traced here: 308 us
  other arithmetic  85.9 us (28%)
  blocking collectives  80.4 us (26%)
  matrix products  54.7 us (18%)
  waiting for transfers between devices  52.2 us (17%)
  local copies, waits for them, and re-layouts  14.9 us (5%)
  between operations  14.7 us (5%)
  starting transfers between devices  4.01 us (1%)
    another operation x5, other arithmetic, block_terms(): jax.scipy.linalg.solve_triangular(identity + lower_part, jnp.broadcast_to...  78.7 us
    all_gather x4, blocking collectives, entering(): lax.all_gather(part.astype(kind), axis)  59.8 us
    dot_general x82, matrix products, high_dot(): return jnp.matmul(left, right, precision=PRECISE)  39.7 us
    reduce_scatter x1, waiting for transfers between devices, on_device(): lax.psum_scatter(term.astype(jnp.bfloat16), 'tp', scatter_dimension=1, ti...  25.1 us
    all_gather x1, blocking collectives, on_device(): lax.all_gather(w_gates, 'sp', axis=0, tiled=True)  14.9 us
    all_gather x1, waiting for transfers between devices, on_device(): lax.all_gather(w_query, 'sp', axis=0, tiled=True)  10.9 us
    dot_general x6, matrix products, on_device(): jnp.dot(normed, rows_here, preferred_element_type=jnp.float32)  10.5 us
    all_gather x1, waiting for transfers between devices, on_device(): lax.all_gather(w_key, 'sp', axis=0, tiled=True)  9.11 us
  transfers between devices with their start and end apart: 8, of which 4 were waited for; matrix products, arithmetic and copies ran while one was open for 48% of the time, Pallas kernels for 0%

commit v1 on v0

--- a/solution.py
+++ b/solution.py
@@ -1,6 +1,10 @@
+import functools
+
 import jax
 import jax.numpy as jnp
 from jax import lax
+from jax.experimental import pallas as pl
+from jax.experimental.pallas import tpu as pltpu
 from jax.sharding import PartitionSpec as P
 
 CONV_CH = 1024
@@ -244,7 +248,501 @@
     return lax.psum_scatter(term.astype(jnp.bfloat16), "tp", scatter_dimension=1, tiled=True)
 
 
+NT = (((1,), (1,)), ((), ()))
+NN = (((1,), (0,)), ((), ()))
+TN = (((0,), (0,)), ((), ()))
+BASE = 16
+VMEM_SPEC = pl.BlockSpec(memory_space=pltpu.VMEM)
+
+
+def mxu(left, right, dims=NN):
+    return lax.dot_general(
+        left.astype(jnp.bfloat16),
+        right.astype(jnp.bfloat16),
+        dims,
+        preferred_element_type=jnp.float32,
+    )
+
+
+def halves(value):
+    high = value.astype(jnp.bfloat16)
+    return high, (value - high.astype(jnp.float32)).astype(jnp.bfloat16)
+
+
+def mxu_fine(left, right, dims=NN):
+    left_high, left_low = halves(left)
+    right_high, right_low = halves(right)
+    return (
+        mxu(left_high, right_high, dims)
+        + mxu(left_high, right_low, dims)
+        + mxu(left_low, right_high, dims)
+    )
+
+
+def call(kernel, out_shape, args, flops=1e8, scratch=(), name=None):
+    return pl.pallas_call(
+        kernel,
+        out_shape=out_shape,
+        in_specs=[VMEM_SPEC] * len(args),
+        out_specs=jax.tree.map(lambda _: VMEM_SPEC, out_shape),
+        scratch_shapes=list(scratch),
+        cost_estimate=pl.CostEstimate(
+            flops=int(flops), bytes_accessed=1 << 20, transcendentals=0
+        ),
+        name=name,
+    )(*args)
+
+
+def norm_kernel(tokens, near, far, gain, normed):
+    place, core = lax.axis_index("sp") % 2, lax.axis_index("tp") % 2
+    rows, width = tokens.shape
+    part = near.shape[1]
+    step = 16
+
+    @pl.loop(0, rows // step)
+    def _(i):
+        here = pl.ds(pl.multiple_of(i * step, step), step)
+        own = tokens[here, :].astype(jnp.float32)
+        scale = lax.rsqrt(jnp.mean(own * own, axis=-1, keepdims=True) + EPSILON)
+        at = pl.ds(pl.multiple_of(place * rows + i * step, step), step)
+        normed[at, :] = (own * scale * gain[...]).astype(jnp.bfloat16)
+        a, b = near[here, :].astype(jnp.float32), far[here, :].astype(jnp.float32)
+        total = jnp.sum(a * a, axis=-1, keepdims=True) + jnp.sum(b * b, axis=-1, keepdims=True)
+        scale = lax.rsqrt(total / width + EPSILON)
+        at = pl.ds(pl.multiple_of((1 - place) * rows + i * step, step), step)
+        for value, which in ((a, core), (b, 1 - core)):
+            columns = pl.ds(pl.multiple_of(which * part, part), part)
+            normed[at, columns] = (value * scale * gain[:, columns]).astype(jnp.bfloat16)
+
+
+def columns_of(normed, shard, half, depth):
+    return normed[:, pl.ds(pl.multiple_of((shard * 2 + half) * depth, depth), depth)]
+
+
+def project(normed, own, crossed, swapped, pick):
+    count = len(crossed) + 1
+    me, copy = lax.axis_index("sp"), lax.axis_index("grp")
+    depth = pick(own).shape[0] // 2
+    whole = normed[:, pl.ds(pl.multiple_of(me * 2 * depth, 2 * depth), 2 * depth)]
+    total = mxu(whole, pick(own))
+    for k in range(1, count):
+        shard = lax.rem(me - k + count, count)
+        for half, pieces in ((copy, crossed), (1 - copy, swapped)):
+            total = total + mxu(
+                columns_of(normed, shard, half, depth), pieces[k - 1][0:depth, :]
+            )
+    return total
+
+
+def substitution(coupling, size, lower):
+    row = lax.broadcasted_iota(jnp.int32, (size, size), 0)
+    lane = lax.broadcasted_iota(jnp.int32, (size, size), 1)
+    same = (row // BASE) == (lane // BASE)
+    diagonal = jnp.where(same, coupling, 0.0)
+    packed = diagonal[0:BASE, :]
+    for k in range(1, size // BASE):
+        packed = packed + diagonal[k * BASE : (k + 1) * BASE, :]
+    tall = jnp.concatenate([packed] * BASE, axis=0)
+    slot = lax.broadcasted_iota(jnp.int32, (BASE * BASE, size), 0) // BASE
+    column = lax.broadcasted_iota(jnp.int32, (BASE * BASE, size), 1) % BASE
+    tall = jnp.where(slot == column, tall, 0.0)
+    ones = jnp.where(same, 1.0, 0.0).astype(jnp.bfloat16)
+    high, low = halves(tall)
+    lowest = (tall - high.astype(jnp.float32) - low.astype(jnp.float32)).astype(jnp.bfloat16)
+    spread = mxu(high, ones) + mxu(low, ones) + mxu(lowest, ones)
+    small_row = lax.broadcasted_iota(jnp.int32, (BASE, size), 0)
+    small_lane = lax.broadcasted_iota(jnp.int32, (BASE, size), 1) % BASE
+    solved = jnp.where(small_row == small_lane, 1.0, 0.0)
+    order = range(BASE - 1) if lower else range(BASE - 1, 0, -1)
+    for j in order:
+        solved = solved - spread[j * BASE : (j + 1) * BASE, :] * solved[j : j + 1, :]
+    return jnp.where(same, jnp.concatenate([solved] * (size // BASE), axis=0), 0.0)
+
+
+def inverse_of(coupling, size, lower):
+    found = substitution(coupling, size, lower)
+    row = lax.broadcasted_iota(jnp.int32, (size, size), 0)
+    lane = lax.broadcasted_iota(jnp.int32, (size, size), 1)
+    width = BASE
+    while width < size:
+        up, left = row // width, lane // width
+        beside = (up // 2 == left // 2) & ((up > left) if lower else (up < left))
+        link = jnp.where(beside, coupling, 0.0)
+        found = found - mxu_fine(found, mxu_fine(link, found))
+        width *= 2
+    return found
+
+
+def unit_rows_of(value):
+    return value * lax.rsqrt(jnp.sum(value * value, axis=-1, keepdims=True) + EPSILON)
+
+
+def silu(value):
+    return value * jax.nn.sigmoid(value)
+
+
+def delta_kernel(others, *refs):
+    normed, w_query, w_key, w_value, gates_own, rates_own, rates_near = refs[:7]
+    crossed, swapped = refs[7 : 7 + others], refs[7 + others : 7 + 2 * others]
+    out, reading, state, gate_rows, rate_rows, table = refs[7 + 2 * others :]
+    me, copy = lax.axis_index("sp"), lax.axis_index("grp")
+    count = others + 1
+    place, late = me % 2, me // 2
+    depth = w_query.shape[0] // 2
+    head = w_query.shape[1] // 2
+    size = rates_own.shape[1]
+    mine = pl.ds(pl.multiple_of(place * head, head), head)
+
+    def pick(own):
+        return jnp.concatenate([w[:, mine] for w in own], axis=1)
+
+    projected = project(normed, (w_query, w_key, w_value), crossed, swapped, pick)
+    whole = normed[:, pl.ds(pl.multiple_of(me * 2 * depth, 2 * depth), 2 * depth)]
+    gates = mxu(gates_own[...], whole, NT)
+    for k in range(1, count):
+        shard = lax.rem(me - k + count, count)
+        for half, pieces in ((copy, crossed), (1 - copy, swapped)):
+            gates = gates + mxu(
+                pieces[k - 1][depth : depth + 16, 0:depth],
+                columns_of(normed, shard, half, depth),
+                NT,
+            )
+    gate_rows[...] = gates
+    for block in range(2):
+        at = slice(block * size, (block + 1) * size)
+        rate_rows[:, at] = jnp.where(place == block, rates_own[...], rates_near[...])
+
+    query = unit_rows_of(silu(projected[:, 0:head])) * head ** (-0.5)
+    keys = unit_rows_of(silu(projected[:, head : 2 * head]))
+    values = silu(projected[:, 2 * head : 3 * head])
+
+    row = lax.broadcasted_iota(jnp.int32, (size, size), 0)
+    lane = lax.broadcasted_iota(jnp.int32, (size, size), 1)
+    table[...] = jnp.zeros_like(table)
+    for d in range(2):
+        decay = rate_rows[pl.ds(2 * place + d, 1), :] * (
+            0.5 + jax.nn.sigmoid(gate_rows[pl.ds(4 * place + 2 * d, 1), :])
+        )
+        rate = jax.nn.sigmoid(gate_rows[pl.ds(4 * place + 2 * d + 1, 1), :] - BETA_SHIFT)
+        summing = (row <= lane) if d == 0 else (row >= lane)
+        summing = jnp.where(summing, 1.0, 0.0).astype(jnp.bfloat16)
+        high, low = halves(decay)
+        lowest = (decay - high.astype(jnp.float32) - low.astype(jnp.float32)).astype(jnp.bfloat16)
+        for block in range(2):
+            at = slice(block * size, (block + 1) * size)
+            table[d : d + 1, at] = sum(
+                mxu(jnp.broadcast_to(part[:, at], (8, size)), summing)[0:1, :]
+                for part in (high, low, lowest)
+            )
+        table[2 + d : 3 + d, :] = rate
+    upright = table[...].T
+
+    solved = []
+    for block in range(2):
+        at = slice(block * size, (block + 1) * size)
+        k, q, v = keys[at], query[at], values[at]
+        alike = mxu_fine(k, k, NT)
+        asked = mxu(q, k, NT)
+        for d in range(2):
+            lower = d == 0
+            sums, sums_row = upright[at, d : d + 1], table[d : d + 1, at]
+            rate = upright[at, 2 + d : 3 + d]
+            reach = (row >= lane) if lower else (row <= lane)
+            weight = jnp.where(reach, jnp.exp(jnp.where(reach, sums - sums_row, 0.0)), 0.0)
+            coupling = jnp.where(row == lane, 0.0, alike * weight) * rate
+            decayed = jnp.exp(sums)
+            inverse = inverse_of(coupling, size, lower)
+            wanted = mxu(inverse, jnp.concatenate([v * rate, k * (rate * decayed)], axis=1))
+            seen = mxu(asked * weight, wanted)
+            last = sums[size - 1 : size] if lower else sums[0:1]
+            pushed = mxu(k * jnp.exp(last - sums), wanted, TN)
+            end_decay = jnp.exp(last)
+            solved.append(
+                (
+                    seen[:, 0:head],
+                    q * decayed - seen[:, head:],
+                    pushed[:, 0:head],
+                    pushed[:, head:],
+                    end_decay,
+                )
+            )
+    results = []
+    for d in range(2):
+        first, second = (solved[d], solved[2 + d]) if d == 0 else (solved[2 + d], solved[d])
+        carried = first[2]
+        later_out = second[0] + mxu(second[1], carried)
+        end = second[2] + second[4] * carried - mxu(second[3], carried)
+        reads = mxu(second[1], first[3])
+        later_read = first[4] * second[1] - reads
+        outs, reads = [first[0], later_out], [first[1], later_read]
+        if d == 1:
+            outs, reads = outs[::-1], reads[::-1]
+        results.append((outs, reads, end))
+    (fore, fore_read, fore_end), (back, back_read, back_end) = results
+    for block in range(2):
+        at = slice(block * size, (block + 1) * size)
+        out[at, :] = fore[block] + back[block]
+        reading[at, :] = jnp.where(late == 1, fore_read[block], back_read[block]).astype(
+            jnp.bfloat16
+        )
+    state[...] = jnp.where(late == 0, fore_end, back_end).astype(jnp.bfloat16)
+
+
+def mix_kernel(local, reading, state, gain, keep, give, whole):
+    place = lax.axis_index("sp") % 2
+    size = local.shape[0] // 2
+    joined = local[...] + mxu(reading[...], state[...])
+    scale = lax.rsqrt(jnp.mean(joined * joined, axis=-1, keepdims=True) + EPSILON)
+    whole[...] = joined * scale * gain[...]
+    keep[...] = whole[pl.ds(pl.multiple_of(place * size, size), size), :].astype(jnp.bfloat16)
+    give[...] = whole[pl.ds(pl.multiple_of((1 - place) * size, size), size), :].astype(
+        jnp.bfloat16
+    )
+
+
+def glu_kernel(others, *refs):
+    normed, w_value, w_gate = refs[:3]
+    crossed, swapped = refs[3 : 3 + others], refs[3 + others : 3 + 2 * others]
+    keep, give, edge_same, edge_other, rows = refs[3 + 2 * others :]
+    place = lax.axis_index("sp") % 2
+    width = w_value.shape[1] // 2
+    mine = pl.ds(pl.multiple_of(place * width, width), width)
+
+    def pick(own):
+        return jnp.concatenate([w[:, mine] for w in own], axis=1)
+
+    projected = project(normed, (w_value, w_gate), crossed, swapped, pick)
+    rows[...] = projected[:, 0:width] * jax.nn.sigmoid(projected[:, width:])
+    halo = edge_same.shape[0]
+    size = keep.shape[0] - halo
+
+    def cut(start, length):
+        return rows[pl.ds(pl.multiple_of(start, halo), length), :].astype(jnp.bfloat16)
+
+    keep[...] = cut(place * (size - halo), size + halo)
+    give[...] = cut((1 - place) * (size - halo), size + halo)
+    edge_same[...] = cut((1 - place) * (2 * size - halo), halo)
+    edge_other[...] = cut(place * (2 * size - halo), halo)
+
+
+def conv_kernel_body(main_same, main_other, edge_same, edge_other, taps, rows, sums, wide):
+    place = lax.axis_index("sp") % 2
+    halo = edge_same.shape[0]
+    size = main_same.shape[0] - halo
+    width = main_same.shape[1]
+    count = taps.shape[0]
+    for main, edge, which in (
+        (main_same, edge_same, place),
+        (main_other, edge_other, 1 - place),
+    ):
+        columns = pl.ds(pl.multiple_of(which * width, width), width)
+        at = pl.ds(pl.multiple_of((1 - place) * halo, halo), size + halo)
+        wide[at, columns] = main[...].astype(jnp.float32)
+        at = pl.ds(pl.multiple_of(place * (size + halo), halo), halo)
+        wide[at, columns] = edge[...].astype(jnp.float32)
+    step = 32
+    for start in range(0, size, step):
+        total = jnp.zeros((step, 2 * width), jnp.float32)
+        for j in range(count):
+            offset = start + halo + j - count // 2
+            total = total + wide[offset : offset + step, :] * taps[j : j + 1, :]
+        rows[start : start + step, :] = total
+    total = rows[...]
+    lane = lax.broadcasted_iota(jnp.int32, (size, 128), 1)
+    sums_tall = jnp.where(
+        lane == 0,
+        jnp.sum(total, axis=-1, keepdims=True),
+        jnp.where(lane == 1, jnp.sum(total * total, axis=-1, keepdims=True), 0.0),
+    )
+    sums[...] = sums_tall.T[0:8, :]
+
+
+def conv_mix_kernel(channels, rows, sums, gain, shift, mixed):
+    size = rows.shape[0]
+    tall = jnp.concatenate([sums[...], jnp.zeros((120, size), jnp.float32)], axis=0).T
+    center = tall[:, 0:1] / channels
+    spread = tall[:, 1:2] / channels - center * center
+    normal = (rows[...] - center) * lax.rsqrt(spread + EPSILON)
+    mixed[...] = silu(normal * gain[...] + shift[...]).astype(jnp.bfloat16)
+
+
+def out_kernel(delta_keep, delta_take, conv_mix, w_delta, w_conv, keep, give, terms):
+    place, core = lax.axis_index("sp") % 2, lax.axis_index("tp") % 2
+    same, take = delta_keep[...], delta_take[...]
+    first = jnp.where(place == 0, same, take)
+    second = jnp.where(place == 0, take, same)
+    left = jnp.concatenate([first, second, conv_mix[...]], axis=1)
+    piece = w_delta.shape[0] // 4
+    for x in range(2):
+        for which, target in ((core, keep), (1 - core, give)):
+            at = pl.ds(pl.multiple_of((2 * x + which) * piece, piece), piece)
+            right = jnp.concatenate([w_delta[at, :], w_conv[at, :]], axis=1)
+            target[:, x * piece : (x + 1) * piece] = mxu(left, right, NT).astype(target.dtype)
+
+
+def swap(value, axis, distance):
+    count = lax.axis_size(axis)
+    return lax.ppermute(value, axis, [(i, i ^ distance) for i in range(count)])
+
+
+def shifted(value, axis, k):
+    count = lax.axis_size(axis)
+    return lax.ppermute(value, axis, [(i, (i + k) % count) for i in range(count)])
+
+
+def paired(
+    tokens_in,
+    input_gain,
+    w_query,
+    w_key,
+    w_value,
+    w_gates,
+    w_glu_value,
+    sigmoid_opener_matrix,
+    log_decay,
+    head_gain,
+    conv_kernel,
+    norm_gain,
+    norm_shift,
+    out_delta,
+    out_conv,
+):
+    count = lax.axis_size("sp")
+    me, copy, tp = lax.axis_index("sp"), lax.axis_index("grp"), lax.axis_index("tp")
+    place = me % 2
+    rows, width = tokens_in.shape
+    head = head_gain.shape[0]
+    depth = w_query.shape[0] // 2
+    bf16, f32 = jnp.bfloat16, jnp.float32
+    shape = jax.ShapeDtypeStruct
+    half_channels = w_glu_value.shape[1] // 2
+
+    gates_tall = jnp.pad(w_gates.T, ((0, 16 - w_gates.shape[1]), (0, 0)))
+    gates_half = lax.dynamic_slice(gates_tall, (0, copy * depth), (16, depth))
+    gates_half = jnp.pad(gates_half, ((0, 0), (0, 3 * head - depth)))
+
+    def message(weights, parity, piece, extra=None):
+        parts = [lax.dynamic_slice(w, (copy * depth, parity * piece), (depth, piece)) for w in weights]
+        whole = jnp.concatenate(parts, axis=1)
+        return whole if extra is None else jnp.concatenate([whole, extra], axis=0)
+
+    delta_weights = (w_query, w_key, w_value)
+    glu_weights = (w_glu_value, sigmoid_opener_matrix)
+    delta_messages = [message(delta_weights, p, head, gates_half) for p in (place, 1 - place)]
+    glu_messages = [message(glu_weights, p, half_channels) for p in (place, 1 - place)]
+    hops = sorted(range(1, count), key=lambda k: (k % 2, k))
+
+    crossed, swapped = {}, {}
+    for k in hops:
+        crossed[k] = shifted(delta_messages[k % 2], "sp", k)
+    part = width // 2
+    near = swap(lax.dynamic_slice(tokens_in, (0, (tp % 2) * part), (rows, part)), "sp", 1)
+    rates = jnp.pad(log_decay.T, ((0, 8 - log_decay.shape[1]), (0, 0)))
+    rates_near = swap(rates, "sp", 1)
+    for k in hops:
+        swapped[k] = swap(crossed[k], "grp", 1)
+    far = swap(near, "tp", 1)
+    glu_crossed = {k: shifted(glu_messages[k % 2], "sp", k) for k in hops}
+    glu_swapped = {k: swap(glu_crossed[k], "grp", 1) for k in hops}
+
+    normed = call(
+        norm_kernel,
+        shape((2 * rows, width), bf16),
+        (tokens_in, near, far, input_gain[None, :]),
+        flops=3e9,
+        name="norm",
+    )
+    order = range(1, count)
+    local, reading, state = call(
+        functools.partial(delta_kernel, count - 1),
+        (shape((2 * rows, head), f32), shape((2 * rows, head), bf16), shape((head, head), bf16)),
+        (normed, w_query, w_key, w_value, gates_tall, rates, rates_near)
+        + tuple(crossed[k] for k in order)
+        + tuple(swapped[k] for k in order),
+        flops=1e10,
+        scratch=(
+            pltpu.VMEM((16, 2 * rows), f32),
+            pltpu.VMEM((8, 2 * rows), f32),
+            pltpu.VMEM((128, 2 * rows), f32),
+        ),
+        name="delta",
+    )
+    state_in = swap(state, "sp", 2)
+    halo = 16
+    keep, give, edge_same, edge_other = call(
+        functools.partial(glu_kernel, count - 1),
+        (shape((rows + halo, half_channels), bf16),) * 2 + (shape((halo, half_channels), bf16),) * 2,
+        (normed, w_glu_value, sigmoid_opener_matrix)
+        + tuple(glu_crossed[k] for k in order)
+        + tuple(glu_swapped[k] for k in order),
+        flops=2e9,
+        scratch=(pltpu.VMEM((2 * rows, half_channels), f32),),
+        name="glu",
+    )
+    taken = swap(give, "sp", 1)
+    outer_same = [(i, i + 2 if i % 2 == 0 else i - 2) for i in range(count)]
+    outer_other = [(i, i - 1 if i % 2 == 0 else i + 1) for i in range(count)]
+    inside = lambda pairs: [(a, b) for a, b in pairs if 0 <= b < count]
+    edge_same = lax.ppermute(edge_same, "sp", inside(outer_same))
+    edge_other = lax.ppermute(edge_other, "sp", inside(outer_other))
+    channels = 2 * half_channels
+    conv_rows, sums = call(
+        conv_kernel_body,
+        (shape((rows, channels), f32), shape((8, rows), f32)),
+        (keep, taken, edge_same, edge_other, conv_kernel),
+        flops=2e9,
+        scratch=(pltpu.VMEM((rows + 2 * halo, channels), f32),),
+        name="conv",
+    )
+    sums = lax.psum(sums, "tp")
+    conv_mix = call(
+        functools.partial(conv_mix_kernel, channels * lax.axis_size("tp")),
+        shape((rows, channels), bf16),
+        (conv_rows, sums, norm_gain[None, :], norm_shift[None, :]),
+        flops=1e9,
+        name="conv_mix",
+    )
+    delta_keep, delta_give = call(
+        mix_kernel,
+        (shape((rows, head), bf16),) * 2,
+        (local, reading, state_in, head_gain[None, :]),
+        flops=1e9,
+        scratch=(pltpu.VMEM((2 * rows, head), f32),),
+        name="mix",
+    )
+    delta_take = swap(delta_give, "sp", 1)
+    features = out_delta.shape[0]
+    keep, give = call(
+        out_kernel,
+        (shape((rows, features // 2), f32), shape((rows, features // 2), bf16)),
+        (delta_keep, delta_take, conv_mix, out_delta, out_conv),
+        flops=2e9,
+        scratch=(pltpu.VMEM((8, 128), f32),),
+        name="out",
+    )
+    both = keep + swap(give, "tp", 1).astype(f32)
+    piece = features // 4
+    x = tp // 2
+    own = lax.dynamic_slice(both, (0, x * piece), (rows, piece))
+    other = lax.dynamic_slice(both, (0, (1 - x) * piece), (rows, piece)).astype(bf16)
+    return (own + swap(other, "tp", 2).astype(f32)).astype(bf16)
+
+
 def solution(mesh):
+    sizes = mesh.shape
+
+    def step(*arguments):
+        tokens_in, w_query, head_gain, conv_kernel = (arguments[i] for i in (0, 2, 9, 10))
+        paired_fits = (
+            (sizes["grp"], sizes["sp"], sizes["tp"]) == (2, 4, 4)
+            and w_query.shape[1] == 2 * head_gain.shape[0]
+            and w_query.shape[0] % 32 == 0
+            and w_query.shape[0] // 2 <= 3 * head_gain.shape[0]
+            and conv_kernel.shape[1] == 2 * head_gain.shape[0]
+            and conv_kernel.shape[0] // 2 < 16
+        )
+        return (paired if paired_fits else on_device)(*arguments)
+
     placed = (
         P(("grp", "sp"), None),
         P(),
@@ -263,5 +761,5 @@
         P(None, "tp"),
     )
     return jax.shard_map(
-        on_device, mesh=mesh, in_specs=placed, out_specs=P(("grp", "sp"), "tp"), check_vma=False
-    )
+        step, mesh=mesh, in_specs=placed, out_specs=P(("grp", "sp"), "tp"), check_vma=False
+    )

time: 309 us -> 127 us (0.41)
  other arithmetic: 85.9 us -> 2.22 us
  blocking collectives: 80.4 us -> 6.43 us
  matrix products: 54.7 us -> 0 us
  Pallas kernels: 0 us -> 37.3 us
  starting transfers between devices: 4.01 us -> 34.6 us
  waiting for transfers between devices: 52.2 us -> 37.5 us
  between operations: 14.7 us -> 0.22 us
  local copies, waits for them, and re-layouts: 14.9 us -> 8.29 us
    another operation x7 -> x0, other arithmetic: 79.7 us -> none  [the longest x5 78.7 us: block_terms(): jax.scipy.linalg.solve_triangular(identity + lower_part, jnp.broadcast_to...]
    all_gather x5 -> x0, blocking collectives: 74.7 us -> none  [the longest x4 59.8 us: entering(): lax.all_gather(part.astype(kind), axis)]
    dot_general x90 -> x0, matrix products: 53.5 us -> none  [the longest x82 39.7 us: high_dot(): return jnp.matmul(left, right, precision=PRECISE)]
    pallas_call x0 -> x7, Pallas kernels: none -> 37.3 us  [call(): pl.pallas_call(kernel, out_shape=out_shape, in_specs=[VMEM_SPEC] * len(ar...]
    ppermute x2 -> x22, waiting for transfers between devices: 3.94 us -> 37.5 us  [the longest x14 30.6 us: swap(): return lax.ppermute(value, axis, [(i, i ^ distance) for i in range(count)])]
    ppermute x2 -> x22, starting transfers between devices: 3.79 us -> 34.6 us  [the longest x14 15.4 us: swap(): return lax.ppermute(value, axis, [(i, i ^ distance) for i in range(count)])]
    reduce_scatter x1 -> x0, waiting for transfers between devices: 25.1 us -> none  [on_device(): lax.psum_scatter(term.astype(jnp.bfloat16), 'tp', scatter_dimension=1, ti...]
    all_gather x5 -> x0, waiting for transfers between devices: 20.1 us -> none  [the longest x1 10.9 us: on_device(): lax.all_gather(w_query, 'sp', axis=0, tiled=True)]
  transfers between devices with their start and end apart: 8 -> 22, of which waited for: 4 -> 8; matrix products, arithmetic and copies ran while one was open for 48% -> 3% of each run, Pallas kernels for 0% -> 27%
where the time goes in v1:
time: 127 us
  waiting for transfers between devices  37.5 us (30%)
  Pallas kernels  37.3 us (29%)
  starting transfers between devices  34.6 us (27%)
  local copies, waits for them, and re-layouts  8.29 us (7%)
  blocking collectives  6.43 us (5%)
  other arithmetic  2.22 us (2%)
    pallas_call x7, Pallas kernels, call(): pl.pallas_call(kernel, out_shape=out_shape, in_specs=[VMEM_SPEC] * len(ar...  37.3 us
    ppermute x14, waiting for transfers between devices, swap(): return lax.ppermute(value, axis, [(i, i ^ distance) for i in range(count)])  30.6 us
    ppermute x14, starting transfers between devices, swap(): return lax.ppermute(value, axis, [(i, i ^ distance) for i in range(count)])  15.4 us
    ppermute x6, starting transfers between devices, shifted(): lax.ppermute(value, axis, [(i, (i + k) % count) for i in range(count)])  13.6 us
    ppermute x6, waiting for transfers between devices, shifted(): lax.ppermute(value, axis, [(i, (i + k) % count) for i in range(count)])  6.93 us
    psum x1, blocking collectives, paired(): sums = lax.psum(sums, 'tp')  6.43 us
    ppermute x1, starting transfers between devices, paired(): edge_same = lax.ppermute(edge_same, 'sp', inside(outer_same))  4.73 us
    unnamed x50, local copies, waits for them, and re-layouts  3.92 us
  transfers between devices with their start and end apart: 22, of which 8 were waited for; matrix products, arithmetic and copies ran while one was open for 3% of the time, Pallas kernels for 27%

profile of v1, /device:TPU:0, one launch (start us, length us, event | category | flops | bytes accessed | tf_op | source)
XLA Modules:
  0.0 126.6 jit_solution(14144030229856092704)
XLA Ops:
  0.0 1.1 constant_dynamic-slice_fusion
  1.1 3.1 %collective-permute-start = (bf16[256,1024]{1,0:T(8,128)(2,1)S(1)}, bf16[256,1024]{1,0:T(8,128)(2,1)S(1)}, u32[]{:S(2)}, u32[]{:S(2)}) collective-permute-start(bf16[256,1024]{1,0:T(8,128)(2,1)S(1)} %constant_dynamic-slice_fusion), channel_id=1, source_target_pairs={{0,4},{4,0},{8,12},{12,8},{1,5},{5,1},{9,13},{13,9},{2,6},{6,2},{1... | collective-permute-start | bytes 1572872 | tf_op jit(solution)/shard_map/ppermute | solution.py:585
  4.3 0.9 fusion.7
  5.2 1.0 fusion.5
  6.2 10.1 %collective-permute-done.near = bf16[256,1024]{1,0:T(8,128)(2,1)S(1)} collective-permute-done((bf16[256,1024]{1,0:T(8,128)(2,1)S(1)}, bf16[256,1024]{1,0:T(8,128)(2,1)S(1)}, u32[]{:S(2)}, u32[]{:S(2)}) %collective-permute-start) | collective-permute-done | bytes 524320 | tf_op jit(solution)/shard_map/ppermute | solution.py:585
  16.2 0.0 collective-permute-start.1
  16.2 0.7 pad_dynamic-slice_fusion
  16.9 0.1 fusion.2
  17.0 1.8 %collective-permute-start.3 = (bf16[272,384]{1,0:T(8,128)(2,1)S(1)}, bf16[272,384]{1,0:T(8,128)(2,1)S(1)}, u32[]{:S(2)}, u32[]{:S(2)}) collective-permute-start(bf16[272,384]{1,0:T(8,128)(2,1)S(1)} %get-tuple-element.42), channel_id=1, source_target_pairs={{0,4},{4,8},{8,12},{12,0},{1,5},{5,9},{9,13},{13,1},{2,6},{6,10},{... | collective-permute-start | bytes 626696 | tf_op jit(solution)/shard_map/ppermute | solution.py:590
  18.8 2.1 %collective-permute-start.5 = (bf16[272,384]{1,0:T(8,128)(2,1)S(1)}, bf16[272,384]{1,0:T(8,128)(2,1)S(1)}, u32[]{:S(2)}, u32[]{:S(2)}) collective-permute-start(bf16[272,384]{1,0:T(8,128)(2,1)S(1)} %get-tuple-element.42), channel_id=1, source_target_pairs={{0,12},{4,0},{8,4},{12,8},{1,13},{5,1},{9,5},{13,9},{2,14},{6,2},{... | collective-permute-start | bytes 626696 | tf_op jit(solution)/shard_map/ppermute | solution.py:590
  20.9 0.1 collective-permute-start.2
  20.9 2.5 %collective-permute-start.4 = (bf16[272,384]{1,0:T(8,128)(2,1)S(1)}, bf16[272,384]{1,0:T(8,128)(2,1)S(1)}, u32[]{:S(2)}, u32[]{:S(2)}) collective-permute-start(bf16[272,384]{1,0:T(8,128)(2,1)S(1)} %get-tuple-element.41), channel_id=1, source_target_pairs={{0,8},{4,12},{8,0},{12,4},{1,9},{5,13},{9,1},{13,5},{2,10},{6,14},... | collective-permute-start | bytes 626696 | tf_op jit(solution)/shard_map/ppermute | solution.py:590
  23.5 7.2 %collective-permute-done.2.refs_6_ = f32[8,256]{1,0:T(8,128)S(1)} collective-permute-done((f32[8,256]{1,0:T(8,128)S(1)}, f32[8,256]{1,0:T(8,128)S(1)}, u32[]{:S(2)}, u32[]{:S(2)}) %collective-permute-start.2) | collective-permute-done | bytes 8224 | tf_op jit(solution)/shard_map/ppermute | solution.py:585
  30.7 0.8 collective-permute-start.11
  31.5 0.6 pad.12.refs_4_
  32.1 6.6 %collective-permute-done.11.refs_3_ = bf16[256,256]{1,0:T(8,128)(2,1)S(1)} collective-permute-done((bf16[256,256]{1,0:T(8,128)(2,1)S(1)}, bf16[256,256]{1,0:T(8,128)(2,1)S(1)}, u32[]{:S(2)}, u32[]{:S(2)}) %collective-permute-start.11) | collective-permute-done | bytes 131104 | tf_op jit(solution)/shard_map/ppermute | solution.py:590
  38.7 3.8 %collective-permute-start.13 = (bf16[256,256]{1,0:T(8,128)(2,1)S(1)}, bf16[256,256]{1,0:T(8,128)(2,1)S(1)}, u32[]{:S(2)}, u32[]{:S(2)}) collective-permute-start(bf16[256,256]{1,0:T(8,128)(2,1)S(1)} %pad_maximum_fusion), channel_id=1, source_target_pairs={{0,12},{4,0},{8,4},{12,8},{1,13},{5,1},{9,5},{13,9},{2,14},{6,2},{... | collective-permute-start | bytes 393224 | tf_op jit(solution)/shard_map/ppermute | solution.py:590
  42.5 0.0 collective-permute-done.3.refs_7_
  42.5 2.7 %collective-permute-start.12 = (bf16[256,256]{1,0:T(8,128)(2,1)S(1)}, bf16[256,256]{1,0:T(8,128)(2,1)S(1)}, u32[]{:S(2)}, u32[]{:S(2)}) collective-permute-start(bf16[256,256]{1,0:T(8,128)(2,1)S(1)} %pad_maximum_fusion.1), channel_id=1, source_target_pairs={{0,8},{4,12},{8,0},{12,4},{1,9},{5,13},{9,1},{13,5},{2,10},{6,14},... | collective-permute-start | bytes 393224 | tf_op jit(solution)/shard_map/ppermute | solution.py:590
  45.1 0.0 collective-permute-done.4.refs_8_
  45.1 1.5 %collective-permute-start.6 = (bf16[272,384]{1,0:T(8,128)(2,1)S(1)}, bf16[272,384]{1,0:T(8,128)(2,1)S(1)}, u32[]{:S(2)}, u32[]{:S(2)}) collective-permute-start(bf16[272,384]{1,0:T(8,128)(2,1)S(1)} %collective-permute-done.3.refs_7_), channel_id=1, source_target_pairs={{0,16},{16,0},{1,17},{17,1},{2,18},{18,2},{3,19},{19,3},{4,20},{20... | collective-permute-start | bytes 626696 | tf_op jit(solution)/shard_map/ppermute | solution.py:585
  46.7 0.0 collective-permute-done.5.refs_9_
  46.7 0.5 collective-permute-start.7
  47.2 0.0 collective-permute-done.1.far
  47.2 1.5 %collective-permute-start.8 = (bf16[272,384]{1,0:T(8,128)(2,1)S(1)}, bf16[272,384]{1,0:T(8,128)(2,1)S(1)}, u32[]{:S(2)}, u32[]{:S(2)}) collective-permute-start(bf16[272,384]{1,0:T(8,128)(2,1)S(1)} %collective-permute-done.5.refs_9_), channel_id=1, source_target_pairs={{0,16},{16,0},{1,17},{17,1},{2,18},{18,2},{3,19},{19,3},{4,20},{20... | collective-permute-start | bytes 626696 | tf_op jit(solution)/shard_map/ppermute | solution.py:585
  48.7 4.9 %norm.1.refs_0_ = bf16[512,2048]{1,0:T(8,128)(2,1)} custom-call(bf16[256,2048]{1,0:T(8,128)(2,1)} %tokens.1, bf16[256,1024]{1,0:T(8,128)(2,1)} %copy-done.5, bf16[256,1024]{1,0:T(8,128)(2,1)} %copy-done.6, f32[1,2048]{1,0:T(1,128)} %bitcast.9), custom_call_target="tpu_custom_call" | custom-call | flops 3000000000 | bytes 1048576 | tf_op jit(solution)/shard_map/norm/pallas_call | solution.py:283
  53.6 0.3 collective-permute-done.12.refs_4_
  54.0 1.5 %collective-permute-start.14 = (bf16[256,256]{1,0:T(8,128)(2,1)S(1)}, bf16[256,256]{1,0:T(8,128)(2,1)S(1)}, u32[]{:S(2)}, u32[]{:S(2)}) collective-permute-start(bf16[256,256]{1,0:T(8,128)(2,1)S(1)} %collective-permute-done.11.refs_3_), channel_id=1, source_target_pairs={{0,16},{16,0},{1,17},{17,1},{2,18},{18,2},{3,19},{19,3},{4,20},{20... | collective-permute-start | bytes 393224 | tf_op jit(solution)/shard_map/ppermute | solution.py:585
  55.5 0.0 collective-permute-done.13.refs_5_
  55.5 0.5 collective-permute-start.15
  56.0 1.5 %collective-permute-start.16 = (bf16[256,256]{1,0:T(8,128)(2,1)S(1)}, bf16[256,256]{1,0:T(8,128)(2,1)S(1)}, u32[]{:S(2)}, u32[]{:S(2)}) collective-permute-start(bf16[256,256]{1,0:T(8,128)(2,1)S(1)} %collective-permute-done.13.refs_5_), channel_id=1, source_target_pairs={{0,16},{16,0},{1,17},{17,1},{2,18},{18,2},{3,19},{19,3},{4,20},{20... | collective-permute-start | bytes 393224 | tf_op jit(solution)/shard_map/ppermute | solution.py:585
  57.5 0.1 collective-permute-done.7.refs_11_
  57.7 4.5 %collective-permute-done.8.refs_12_ = bf16[272,384]{1,0:T(8,128)(2,1)S(1)} collective-permute-done((bf16[272,384]{1,0:T(8,128)(2,1)S(1)}, bf16[272,384]{1,0:T(8,128)(2,1)S(1)}, u32[]{:S(2)}, u32[]{:S(2)}) %collective-permute-start.8) | collective-permute-done | bytes 208928 | tf_op jit(solution)/shard_map/ppermute | solution.py:585
  62.2 0.7 copy-done.12
  62.9 18.6 %delta.1 = (f32[512,128]{1,0:T(8,128)}, bf16[512,128]{1,0:T(8,128)(2,1)}, bf16[128,128]{1,0:T(8,128)(2,1)}) custom-call(bf16[512,2048]{1,0:T(8,128)(2,1)} %norm.1.refs_0_, bf16[512,256]{1,0:T(8,128)(2,1)} %refs_1_.2, bf16[512,256]{1,0:T(8,128)(2,1)} %refs_2_.2, bf16[512,256]{1,0:T(8,128)(2,1)} %refs_3_.1, bf16[16,512]{1,0:T(8,128)(2,1)} %pad.12.refs_4_, ...), custom_call_target="tpu_custom_call" | custom-call | flops 10000000000 | bytes 1048576 | tf_op jit(solution)/shard_map/delta/pallas_call | solution.py:283
  81.5 0.3 collective-permute-start.9
  81.8 0.0 collective-permute-done.14.refs_6_
  81.8 0.0 collective-permute-done.15.refs_7_
  81.9 0.6 copy-done.16
  82.5 0.1 copy-done.17
  82.5 0.6 copy-done.18
  83.2 3.4 %glu.1 = (bf16[272,128]{1,0:T(8,128)(2,1)}, bf16[272,128]{1,0:T(8,128)(2,1)}, bf16[16,128]{1,0:T(8,128)(2,1)}, bf16[16,128]{1,0:T(8,128)(2,1)}) custom-call(bf16[512,2048]{1,0:T(8,128)(2,1)} %norm.1.refs_0_, bf16[512,256]{1,0:T(8,128)(2,1)} %refs_1_.3, bf16[512,256]{1,0:T(8,128)(2,1)} %refs_2_.3, bf16[256,256]{1,0:T(8,128)(2,1)} %copy-done.13, ...), custom_call_target="tpu_custom_call" | custom-call | flops 2000000000 | bytes 1048576 | tf_op jit(solution)/shard_map/glu/pallas_call | solution.py:283
  86.6 1.8 %collective-permute-start.17 = (bf16[272,128]{1,0:T(8,128)(2,1)}, bf16[272,128]{1,0:T(8,128)(2,1)S(1)}, u32[]{:S(2)}, u32[]{:S(2)}) collective-permute-start(bf16[272,128]{1,0:T(8,128)(2,1)} %get-tuple-element.24), channel_id=1, source_target_pairs={{0,4},{4,0},{8,12},{12,8},{1,5},{5,1},{9,13},{13,9},{2,6},{6,2},{1... | collective-permute-start | bytes 208904 | tf_op jit(solution)/shard_map/ppermute | solution.py:585
  88.4 4.7 %collective-permute-start.18 = (bf16[16,128]{1,0:T(8,128)(2,1)}, bf16[16,128]{1,0:T(8,128)(2,1)S(1)}, u32[]{:S(2)}, u32[]{:S(2)}) collective-permute-start(bf16[16,128]{1,0:T(8,128)(2,1)} %get-tuple-element.25), channel_id=1, source_target_pairs={{0,8},{12,4},{1,9},{13,5},{2,10},{14,6},{3,11},{15,7},{16,24},{28,... | collective-permute-start | bytes 12296 | tf_op jit(solution)/shard_map/ppermute | solution.py:686
  93.1 0.8 collective-permute-start.19
  94.0 0.6 copy-done.21
  94.6 2.0 %mix.1 = (bf16[256,128]{1,0:T(8,128)(2,1)}, bf16[256,128]{1,0:T(8,128)(2,1)}) custom-call(f32[512,128]{1,0:T(8,128)} %get-tuple-element.18.local, bf16[512,128]{1,0:T(8,128)(2,1)} %get-tuple-element.19.reading, bf16[128,128]{1,0:T(8,128)(2,1)} %copy-done.21, f32[1,128]{1,0:T(1,128)} %bitcast.12), custom_call_target="tpu_custom_call" | custom-call | flops 1000000000 | bytes 1048576 | tf_op jit(solution)/shard_map/mix/pallas_call | solution.py:283
  96.6 1.2 collective-permute-start.10
  97.8 0.0 collective-permute-done.18.edge_same
  97.8 0.0 collective-permute-done.19.edge_other
  97.8 0.6 copy-done.23
  98.4 0.0 copy-done.24
  98.4 0.1 copy-done.19
  98.4 3.0 %conv.1 = (f32[256,256]{1,0:T(8,128)}, f32[8,256]{1,0:T(8,128)}) custom-call(bf16[272,128]{1,0:T(8,128)(2,1)} %get-tuple-element.23.main_same, bf16[272,128]{1,0:T(8,128)(2,1)} %copy-done.19, bf16[16,128]{1,0:T(8,128)(2,1)} %copy-done.23, bf16[16,128]{1,0:T(8,128)(2,1)} %copy-done.24, f32[31,256]{1,0:T(8,128)} %taps.1), custom_call_target="tpu_custom_call" | custom-call | flops 2000000000 | bytes 1048576 | tf_op jit(solution)/shard_map/conv/pallas_call | solution.py:283
  101.4 6.4 %psum.7.sums = f32[8,256]{1,0:T(8,128)} all-reduce(f32[8,256]{1,0:T(8,128)} %get-tuple-element.28), channel_id=1, replica_groups=mesh['grp'=2,'sp'=4,'tp'=4] {'tp'}, use_global_device_ids=true, to_apply=%region_0.1 | all-reduce | flops 2048 | bytes 16384 | tf_op jit(solution)/shard_map/psum | solution.py:697
  107.8 2.0 %conv_mix.1 = bf16[256,256]{1,0:T(8,128)(2,1)} custom-call(f32[256,256]{1,0:T(8,128)} %get-tuple-element.27.rows, f32[8,256]{1,0:T(8,128)} %psum.7.sums, f32[1,256]{1,0:T(1,128)} %bitcast.10, f32[1,256]{1,0:T(1,128)} %bitcast.11), custom_call_target="tpu_custom_call" | custom-call | flops 1000000000 | bytes 1048576 | tf_op jit(solution)/shard_map/conv_mix/pallas_call | solution.py:283
  109.8 0.0 collective-permute-done.10.delta_take
  109.8 0.6 copy-done.20
  110.4 3.4 %out.1 = (f32[256,1024]{1,0:T(8,128)}, bf16[256,1024]{1,0:T(8,128)(2,1)}) custom-call(bf16[256,128]{1,0:T(8,128)(2,1)} %get-tuple-element.21.delta_keep, bf16[256,128]{1,0:T(8,128)(2,1)} %copy-done.20, bf16[256,256]{1,0:T(8,128)(2,1)} %conv_mix.1, bf16[2048,256]{1,0:T(8,128)(2,1)} %w_delta.1, bf16[2048,256]{1,0:T(8,128)(2,1)} %w_conv.1), custom_call_target="tpu_custom_call" | custom-call | flops 2000000000 | bytes 1048576 | tf_op jit(solution)/shard_map/out/pallas_call | solution.py:283
  113.9 2.1 %collective-permute-done.20 = bf16[256,1024]{1,0:T(8,128)(2,1)S(1)} collective-permute-done((bf16[256,1024]{1,0:T(8,128)(2,1)}, bf16[256,1024]{1,0:T(8,128)(2,1)S(1)}, u32[]{:S(2)}, u32[]{:S(2)}) %collective-permute-start.20) | collective-permute-done | bytes 524320 | tf_op jit(solution)/shard_map/ppermute | solution.py:585
  116.0 1.4 %convert_add_fusion = f32[256,1024]{1,0:T(8,128)S(1)} fusion(f32[256,1024]{1,0:T(8,128)} %get-tuple-element.29, bf16[256,1024]{1,0:T(8,128)(2,1)S(1)} %collective-permute-done.20), kind=kLoop, calls=%fused_computation | loop fusion | flops 524288 | bytes 2621440 | tf_op jit(solution)/shard_map/add | solution.py:723
  117.4 1.8 %collective-permute-start.21 = (bf16[256,512]{1,0:T(8,128)(2,1)S(1)}, bf16[256,512]{1,0:T(8,128)(2,1)S(1)}, u32[]{:S(2)}, u32[]{:S(2)}) collective-permute-start(bf16[256,512]{1,0:T(8,128)(2,1)S(1)} %dynamic-slice_convert_fusion), channel_id=1, source_target_pairs={{0,2},{1,3},{2,0},{3,1},{4,6},{5,7},{6,4},{7,5},{8,10},{9,11},{10,... | collective-permute-start | bytes 786440 | tf_op jit(solution)/shard_map/ppermute | solution.py:585
  119.2 6.6 %collective-permute-done.21 = bf16[256,512]{1,0:T(8,128)(2,1)S(1)} collective-permute-done((bf16[256,512]{1,0:T(8,128)(2,1)S(1)}, bf16[256,512]{1,0:T(8,128)(2,1)S(1)}, u32[]{:S(2)}, u32[]{:S(2)}) %collective-permute-start.21) | collective-permute-done | bytes 262176 | tf_op jit(solution)/shard_map/ppermute | solution.py:585
  125.8 0.8 add_convert_fusion
  (51 shorter events, 0.2 us)
Async XLA Ops:
  0.0 31.5 %copy-start.2 = (bf16[512,8]{0,1:T(8,128)(2,1)S(1)}, bf16[512,8]{0,1:T(8,128)(2,1)}, u32[]{:S(2)}) copy-start(bf16[512,8]{0,1:T(8,128)(2,1)} %param.20) | copy-start | bytes 24580
  0.0 20.9 %copy-start.4 = (f32[256,4]{0,1:T(4,128)S(1)}, f32[256,4]{0,1:T(4,128)}, u32[]{:S(2)}) copy-start(f32[256,4]{0,1:T(4,128)} %param.23) | copy-start | bytes 12292
  0.0 23.5 %copy-start = (bf16[512,256]{1,0:T(8,128)(2,1)S(1)}, bf16[512,256]{1,0:T(8,128)(2,1)}, u32[]{:S(2)}) copy-start(bf16[512,256]{1,0:T(8,128)(2,1)} %refs_1_.3) | copy-start | bytes 786436
  0.0 23.5 %copy-start.1 = (bf16[512,256]{1,0:T(8,128)(2,1)S(1)}, bf16[512,256]{1,0:T(8,128)(2,1)}, u32[]{:S(2)}) copy-start(bf16[512,256]{1,0:T(8,128)(2,1)} %refs_2_.3) | copy-start | bytes 786436
  1.1 15.1 %collective-permute-start = (bf16[256,1024]{1,0:T(8,128)(2,1)S(1)}, bf16[256,1024]{1,0:T(8,128)(2,1)S(1)}, u32[]{:S(2)}, u32[]{:S(2)}) collective-permute-start(bf16[256,1024]{1,0:T(8,128)(2,1)S(1)} %constant_dynamic-slice_fusion), channel_id=1, source_target_pairs={{0,4},{4,0},{8,12},{12,8},{1,5},{5,1},{9,13},{13,9},{2,6},{6,2},{1... | collective-permute-start | bytes 1572872 | tf_op jit(solution)/shard_map/ppermute | solution.py:585
  16.2 32.5 %copy-start.5 = (bf16[256,1024]{1,0:T(8,128)(2,1)}, bf16[256,1024]{1,0:T(8,128)(2,1)S(1)}, u32[]{:S(2)}) copy-start(bf16[256,1024]{1,0:T(8,128)(2,1)S(1)} %collective-permute-done.near) | copy-start | bytes 1572868
  16.2 30.9 %collective-permute-start.1 = (bf16[256,1024]{1,0:T(8,128)(2,1)S(1)}, bf16[256,1024]{1,0:T(8,128)(2,1)S(1)}, u32[]{:S(2)}, u32[]{:S(2)}) collective-permute-start(bf16[256,1024]{1,0:T(8,128)(2,1)S(1)} %collective-permute-done.near), channel_id=1, source_target_pairs={{0,1},{1,0},{2,3},{3,2},{4,5},{5,4},{6,7},{7,6},{8,9},{9,8},{10,11... | collective-permute-start | bytes 1572872 | tf_op jit(solution)/shard_map/ppermute | solution.py:585
  17.0 25.5 %collective-permute-start.3 = (bf16[272,384]{1,0:T(8,128)(2,1)S(1)}, bf16[272,384]{1,0:T(8,128)(2,1)S(1)}, u32[]{:S(2)}, u32[]{:S(2)}) collective-permute-start(bf16[272,384]{1,0:T(8,128)(2,1)S(1)} %get-tuple-element.42), channel_id=1, source_target_pairs={{0,4},{4,8},{8,12},{12,0},{1,5},{5,9},{9,13},{13,1},{2,6},{6,10},{... | collective-permute-start | bytes 626696 | tf_op jit(solution)/shard_map/ppermute | solution.py:590
  18.8 27.9 %collective-permute-start.5 = (bf16[272,384]{1,0:T(8,128)(2,1)S(1)}, bf16[272,384]{1,0:T(8,128)(2,1)S(1)}, u32[]{:S(2)}, u32[]{:S(2)}) collective-permute-start(bf16[272,384]{1,0:T(8,128)(2,1)S(1)} %get-tuple-element.42), channel_id=1, source_target_pairs={{0,12},{4,0},{8,4},{12,8},{1,13},{5,1},{9,5},{13,9},{2,14},{6,2},{... | collective-permute-start | bytes 626696 | tf_op jit(solution)/shard_map/ppermute | solution.py:590
  20.9 32.8 %copy-start.3 = (f32[8,256]{1,0:T(8,128)}, f32[8,256]{1,0:T(8,128)S(1)}, u32[]{:S(2)}) copy-start(f32[8,256]{1,0:T(8,128)S(1)} %pad.13.refs_5_) | copy-start | bytes 24580
  20.9 9.8 %collective-permute-start.2 = (f32[8,256]{1,0:T(8,128)S(1)}, f32[8,256]{1,0:T(8,128)S(1)}, u32[]{:S(2)}, u32[]{:S(2)}) collective-permute-start(f32[8,256]{1,0:T(8,128)S(1)} %pad.13.refs_5_), channel_id=1, source_target_pairs={{0,4},{4,0},{8,12},{12,8},{1,5},{5,1},{9,13},{13,9},{2,6},{6,2},{1... | collective-permute-start | bytes 24584 | tf_op jit(solution)/shard_map/ppermute | solution.py:585
  20.9 24.2 %collective-permute-start.4 = (bf16[272,384]{1,0:T(8,128)(2,1)S(1)}, bf16[272,384]{1,0:T(8,128)(2,1)S(1)}, u32[]{:S(2)}, u32[]{:S(2)}) collective-permute-start(bf16[272,384]{1,0:T(8,128)(2,1)S(1)} %get-tuple-element.41), channel_id=1, source_target_pairs={{0,8},{4,12},{8,0},{12,4},{1,9},{5,13},{9,1},{13,5},{2,10},{6,14},... | collective-permute-start | bytes 626696 | tf_op jit(solution)/shard_map/ppermute | solution.py:590
  30.7 22.9 %copy-start.22 = (f32[8,256]{1,0:T(8,128)}, f32[8,256]{1,0:T(8,128)S(1)}, u32[]{:S(2)}) copy-start(f32[8,256]{1,0:T(8,128)S(1)} %collective-permute-done.2.refs_6_) | copy-start | bytes 24580
  30.7 8.0 %collective-permute-start.11 = (bf16[256,256]{1,0:T(8,128)(2,1)S(1)}, bf16[256,256]{1,0:T(8,128)(2,1)S(1)}, u32[]{:S(2)}, u32[]{:S(2)}) collective-permute-start(bf16[256,256]{1,0:T(8,128)(2,1)S(1)} %pad_maximum_fusion), channel_id=1, source_target_pairs={{0,4},{4,8},{8,12},{12,0},{1,5},{5,9},{9,13},{13,1},{2,6},{6,10},{... | collective-permute-start | bytes 393224 | tf_op jit(solution)/shard_map/ppermute | solution.py:590
  38.7 42.8 %copy-start.13 = (bf16[256,256]{1,0:T(8,128)(2,1)}, bf16[256,256]{1,0:T(8,128)(2,1)S(1)}, u32[]{:S(2)}) copy-start(bf16[256,256]{1,0:T(8,128)(2,1)S(1)} %collective-permute-done.11.refs_3_) | copy-start | bytes 393220
  38.7 16.8 %collective-permute-start.13 = (bf16[256,256]{1,0:T(8,128)(2,1)S(1)}, bf16[256,256]{1,0:T(8,128)(2,1)S(1)}, u32[]{:S(2)}, u32[]{:S(2)}) collective-permute-start(bf16[256,256]{1,0:T(8,128)(2,1)S(1)} %pad_maximum_fusion), channel_id=1, source_target_pairs={{0,12},{4,0},{8,4},{12,8},{1,13},{5,1},{9,5},{13,9},{2,14},{6,2},{... | collective-permute-start | bytes 393224 | tf_op jit(solution)/shard_map/ppermute | solution.py:590
  42.5 19.7 %copy-start.7 = (bf16[272,384]{1,0:T(8,128)(2,1)}, bf16[272,384]{1,0:T(8,128)(2,1)S(1)}, u32[]{:S(2)}) copy-start(bf16[272,384]{1,0:T(8,128)(2,1)S(1)} %collective-permute-done.3.refs_7_) | copy-start | bytes 626692
  42.5 11.5 %collective-permute-start.12 = (bf16[256,256]{1,0:T(8,128)(2,1)S(1)}, bf16[256,256]{1,0:T(8,128)(2,1)S(1)}, u32[]{:S(2)}, u32[]{:S(2)}) collective-permute-start(bf16[256,256]{1,0:T(8,128)(2,1)S(1)} %pad_maximum_fusion.1), channel_id=1, source_target_pairs={{0,8},{4,12},{8,0},{12,4},{1,9},{5,13},{9,1},{13,5},{2,10},{6,14},... | collective-permute-start | bytes 393224 | tf_op jit(solution)/shard_map/ppermute | solution.py:590
  45.1 17.0 %copy-start.9 = (bf16[272,384]{1,0:T(8,128)(2,1)}, bf16[272,384]{1,0:T(8,128)(2,1)S(1)}, u32[]{:S(2)}) copy-start(bf16[272,384]{1,0:T(8,128)(2,1)S(1)} %collective-permute-done.4.refs_8_) | copy-start | bytes 626692
  45.1 10.9 %collective-permute-start.6 = (bf16[272,384]{1,0:T(8,128)(2,1)S(1)}, bf16[272,384]{1,0:T(8,128)(2,1)S(1)}, u32[]{:S(2)}, u32[]{:S(2)}) collective-permute-start(bf16[272,384]{1,0:T(8,128)(2,1)S(1)} %collective-permute-done.3.refs_7_), channel_id=1, source_target_pairs={{0,16},{16,0},{1,17},{17,1},{2,18},{18,2},{3,19},{19,3},{4,20},{20... | collective-permute-start | bytes 626696 | tf_op jit(solution)/shard_map/ppermute | solution.py:585
  46.7 15.5 %copy-start.8 = (bf16[272,384]{1,0:T(8,128)(2,1)}, bf16[272,384]{1,0:T(8,128)(2,1)S(1)}, u32[]{:S(2)}) copy-start(bf16[272,384]{1,0:T(8,128)(2,1)S(1)} %collective-permute-done.5.refs_9_) | copy-start | bytes 626692
  46.7 11.0 %collective-permute-start.7 = (bf16[272,384]{1,0:T(8,128)(2,1)S(1)}, bf16[272,384]{1,0:T(8,128)(2,1)S(1)}, u32[]{:S(2)}, u32[]{:S(2)}) collective-permute-start(bf16[272,384]{1,0:T(8,128)(2,1)S(1)} %collective-permute-done.4.refs_8_), channel_id=1, source_target_pairs={{0,16},{16,0},{1,17},{17,1},{2,18},{18,2},{3,19},{19,3},{4,20},{20... | collective-permute-start | bytes 626696 | tf_op jit(solution)/shard_map/ppermute | solution.py:585
  47.2 1.5 %copy-start.6 = (bf16[256,1024]{1,0:T(8,128)(2,1)}, bf16[256,1024]{1,0:T(8,128)(2,1)S(1)}, u32[]{:S(2)}) copy-start(bf16[256,1024]{1,0:T(8,128)(2,1)S(1)} %collective-permute-done.1.far) | copy-start | bytes 1572868
  47.2 15.0 %collective-permute-start.8 = (bf16[272,384]{1,0:T(8,128)(2,1)S(1)}, bf16[272,384]{1,0:T(8,128)(2,1)S(1)}, u32[]{:S(2)}, u32[]{:S(2)}) collective-permute-start(bf16[272,384]{1,0:T(8,128)(2,1)S(1)} %collective-permute-done.5.refs_9_), channel_id=1, source_target_pairs={{0,16},{16,0},{1,17},{17,1},{2,18},{18,2},{3,19},{19,3},{4,20},{20... | collective-permute-start | bytes 626696 | tf_op jit(solution)/shard_map/ppermute | solution.py:585
  54.0 27.5 %copy-start.15 = (bf16[256,256]{1,0:T(8,128)(2,1)}, bf16[256,256]{1,0:T(8,128)(2,1)S(1)}, u32[]{:S(2)}) copy-start(bf16[256,256]{1,0:T(8,128)(2,1)S(1)} %collective-permute-done.12.refs_4_) | copy-start | bytes 393220
  54.0 27.9 %collective-permute-start.14 = (bf16[256,256]{1,0:T(8,128)(2,1)S(1)}, bf16[256,256]{1,0:T(8,128)(2,1)S(1)}, u32[]{:S(2)}, u32[]{:S(2)}) collective-permute-start(bf16[256,256]{1,0:T(8,128)(2,1)S(1)} %collective-permute-done.11.refs_3_), channel_id=1, source_target_pairs={{0,16},{16,0},{1,17},{17,1},{2,18},{18,2},{3,19},{19,3},{4,20},{20... | collective-permute-start | bytes 393224 | tf_op jit(solution)/shard_map/ppermute | solution.py:585
  55.5 26.0 %copy-start.14 = (bf16[256,256]{1,0:T(8,128)(2,1)}, bf16[256,256]{1,0:T(8,128)(2,1)S(1)}, u32[]{:S(2)}) copy-start(bf16[256,256]{1,0:T(8,128)(2,1)S(1)} %collective-permute-done.13.refs_5_) | copy-start | bytes 393220
  55.5 26.3 %collective-permute-start.15 = (bf16[256,256]{1,0:T(8,128)(2,1)S(1)}, bf16[256,256]{1,0:T(8,128)(2,1)S(1)}, u32[]{:S(2)}, u32[]{:S(2)}) collective-permute-start(bf16[256,256]{1,0:T(8,128)(2,1)S(1)} %collective-permute-done.12.refs_4_), channel_id=1, source_target_pairs={{0,16},{16,0},{1,17},{17,1},{2,18},{18,2},{3,19},{19,3},{4,20},{20... | collective-permute-start | bytes 393224 | tf_op jit(solution)/shard_map/ppermute | solution.py:585
  56.0 6.1 %copy-start.10 = (bf16[272,384]{1,0:T(8,128)(2,1)}, bf16[272,384]{1,0:T(8,128)(2,1)S(1)}, u32[]{:S(2)}) copy-start(bf16[272,384]{1,0:T(8,128)(2,1)S(1)} %collective-permute-done.6.refs_10_) | copy-start | bytes 626692
  56.0 25.8 %collective-permute-start.16 = (bf16[256,256]{1,0:T(8,128)(2,1)S(1)}, bf16[256,256]{1,0:T(8,128)(2,1)S(1)}, u32[]{:S(2)}, u32[]{:S(2)}) collective-permute-start(bf16[256,256]{1,0:T(8,128)(2,1)S(1)} %collective-permute-done.13.refs_5_), channel_id=1, source_target_pairs={{0,16},{16,0},{1,17},{17,1},{2,18},{18,2},{3,19},{19,3},{4,20},{20... | collective-permute-start | bytes 393224 | tf_op jit(solution)/shard_map/ppermute | solution.py:585
  57.7 4.5 %copy-start.11 = (bf16[272,384]{1,0:T(8,128)(2,1)}, bf16[272,384]{1,0:T(8,128)(2,1)S(1)}, u32[]{:S(2)}) copy-start(bf16[272,384]{1,0:T(8,128)(2,1)S(1)} %collective-permute-done.7.refs_11_) | copy-start | bytes 626692
  62.2 0.7 copy-start.12
  81.5 12.4 %collective-permute-start.9 = (bf16[128,128]{1,0:T(8,128)(2,1)}, bf16[128,128]{1,0:T(8,128)(2,1)S(1)}, u32[]{:S(2)}, u32[]{:S(2)}) collective-permute-start(bf16[128,128]{1,0:T(8,128)(2,1)} %get-tuple-element.20), channel_id=1, source_target_pairs={{0,8},{4,12},{8,0},{12,4},{1,9},{5,13},{9,1},{13,5},{2,10},{6,14},... | collective-permute-start | bytes 98312 | tf_op jit(solution)/shard_map/ppermute | solution.py:585
  81.8 0.7 copy-start.16
  81.8 0.7 copy-start.17
  82.5 0.7 copy-start.18
  86.6 11.2 %collective-permute-start.17 = (bf16[272,128]{1,0:T(8,128)(2,1)}, bf16[272,128]{1,0:T(8,128)(2,1)S(1)}, u32[]{:S(2)}, u32[]{:S(2)}) collective-permute-start(bf16[272,128]{1,0:T(8,128)(2,1)} %get-tuple-element.24), channel_id=1, source_target_pairs={{0,4},{4,0},{8,12},{12,8},{1,5},{5,1},{9,13},{13,9},{2,6},{6,2},{1... | collective-permute-start | bytes 208904 | tf_op jit(solution)/shard_map/ppermute | solution.py:585
  88.4 9.4 %collective-permute-start.18 = (bf16[16,128]{1,0:T(8,128)(2,1)}, bf16[16,128]{1,0:T(8,128)(2,1)S(1)}, u32[]{:S(2)}, u32[]{:S(2)}) collective-permute-start(bf16[16,128]{1,0:T(8,128)(2,1)} %get-tuple-element.25), channel_id=1, source_target_pairs={{0,8},{12,4},{1,9},{13,5},{2,10},{14,6},{3,11},{15,7},{16,24},{28,... | collective-permute-start | bytes 12296 | tf_op jit(solution)/shard_map/ppermute | solution.py:686
  93.1 4.7 %collective-permute-start.19 = (bf16[16,128]{1,0:T(8,128)(2,1)}, bf16[16,128]{1,0:T(8,128)(2,1)S(1)}, u32[]{:S(2)}, u32[]{:S(2)}) collective-permute-start(bf16[16,128]{1,0:T(8,128)(2,1)} %get-tuple-element.26), channel_id=1, source_target_pairs={{4,8},{8,4},{5,9},{9,5},{6,10},{10,6},{7,11},{11,7},{20,24},{24,20... | collective-permute-start | bytes 12296 | tf_op jit(solution)/shard_map/ppermute | solution.py:687
  94.0 0.6 copy-start.21
  96.6 13.3 %collective-permute-start.10 = (bf16[256,128]{1,0:T(8,128)(2,1)}, bf16[256,128]{1,0:T(8,128)(2,1)S(1)}, u32[]{:S(2)}, u32[]{:S(2)}) collective-permute-start(bf16[256,128]{1,0:T(8,128)(2,1)} %get-tuple-element.22), channel_id=1, source_target_pairs={{0,4},{4,0},{8,12},{12,8},{1,5},{5,1},{9,13},{13,9},{2,6},{6,2},{1... | collective-permute-start | bytes 196616 | tf_op jit(solution)/shard_map/ppermute | solution.py:585
  97.8 0.6 copy-start.23
  97.8 0.6 copy-start.24
  97.8 0.6 copy-start.19
  109.8 0.6 copy-start.20
  113.9 2.1 %collective-permute-start.20 = (bf16[256,1024]{1,0:T(8,128)(2,1)}, bf16[256,1024]{1,0:T(8,128)(2,1)S(1)}, u32[]{:S(2)}, u32[]{:S(2)}) collective-permute-start(bf16[256,1024]{1,0:T(8,128)(2,1)} %get-tuple-element.30), channel_id=1, source_target_pairs={{0,1},{1,0},{2,3},{3,2},{4,5},{5,4},{6,7},{7,6},{8,9},{9,8},{10,11... | collective-permute-start | bytes 1572872 | tf_op jit(solution)/shard_map/ppermute | solution.py:585
  117.4 8.4 %collective-permute-start.21 = (bf16[256,512]{1,0:T(8,128)(2,1)S(1)}, bf16[256,512]{1,0:T(8,128)(2,1)S(1)}, u32[]{:S(2)}, u32[]{:S(2)}) collective-permute-start(bf16[256,512]{1,0:T(8,128)(2,1)S(1)} %dynamic-slice_convert_fusion), channel_id=1, source_target_pairs={{0,2},{1,3},{2,0},{3,1},{4,6},{5,7},{6,4},{7,5},{8,10},{9,11},{10,... | collective-permute-start | bytes 786440 | tf_op jit(solution)/shard_map/ppermute | solution.py:585
